TPU v7x, 256 devices: a whole 4x4x8 slice. The times are simulated.
256 devices in a mesh: ep: 64 (over z, x, core), tp: 4 (over y).
Axes of the slice: x: 4, y: 4, z: 8, core: 2. Of those that a mesh axis runs over, the one named last changes fastest.
Arguments:
- tokens: bfloat16 [512, 2048], P('ep'), may hold values from -6 to 6
- lengths: int32 [512], P('ep'), may hold values from 1 to 1024, as said below
- cache_keys: bfloat16 [512, 4, 1024, 128], P('ep', 'tp'), may hold values from -120 to 120
- cache_values: bfloat16 [512, 4, 1024, 128], P('ep', 'tp'), may hold values from -6 to 6
- w_query: bfloat16 [2048, 2048], P('ep', 'tp'), may hold values from -0.21875 to 0.21875
- w_key: bfloat16 [2048, 512], P('ep', 'tp'), may hold values from -0.125 to 0.125
- w_value: bfloat16 [2048, 512], P('ep', 'tp'), may hold values from -0.125 to 0.125
- mix_weight: float32 [16], P('tp'), may hold values from 0.3 to 0.8
- head_gain: float32 [128], replicated, may hold values from 0.1 to 1.9
- w_out: bfloat16 [2048, 2048], P('tp', 'ep'), may hold values from -0.125 to 0.125
- first_gain: float32 [2048], replicated, may hold values from 0.1 to 1.9
- routing: int32 [512, 2], P('ep'), may hold values from 0 to 15, all different within a row; in each aligned block of 8 rows (0 to 7, 8 to 15, ...) at most 2 rows name the same one
- route_weights: float32 [512, 2], P('ep'), may hold values from 0.1 to 0.9
- expert_gate: bfloat16 [64, 2048, 1408], P('ep', None, 'tp'), may hold values from -0.125 to 0.125
- expert_up: bfloat16 [64, 2048, 1408], P('ep', None, 'tp'), may hold values from -0.125 to 0.125
- expert_down: bfloat16 [64, 1408, 2048], P('ep', None, 'tp'), may hold values from -0.078125 to 0.078125
- dense_gate: bfloat16 [2048, 4096], P('tp', 'ep'), may hold values from -0.125 to 0.125
- dense_up: bfloat16 [2048, 4096], P('tp', 'ep'), may hold values from -0.125 to 0.125
- dense_down: bfloat16 [4096, 2048], P('ep', 'tp'), may hold values from -0.09375 to 0.09375
- switch_vector: float32 [2048], replicated, may hold values from -0.25 to 0.25
- final_gain: float32 [2048], P('tp'), may hold values from 0.1 to 1.9
Outputs:
- mixed: bfloat16 [512, 2048], P('ep', 'tp')
Inputs may be any that keep to these rules, and one draw needn't show every extreme that they name: `lengths`: every sequence has at least one cached position; some sequence has exactly 1024. `routing`: each row names 2 different experts; among the rows of one index of ep no expert is named more than 2 times, a bound that some block reaches.
All inputs are finite; a program needn't handle non-finite values.
Results may differ from a plain program's by a relative error of at most 0.015.
The roundings to bfloat16 on the way count: a program that leaves them out, or rounds other values in their place, can miss the bound.
Values may be sent and summed in bfloat16 or wider, within the bound.
A program may use at most 64 MiB of HBM per device.

v0:
```python
import jax
import jax.numpy as jnp
from jax import lax
from jax.sharding import PartitionSpec as P

QK = 128
HEAD = 64
SPAN = 4
TOP = 2


EPS = 1e-05


def in_one_piece(arrays, axis, dim, along):
    both = jnp.concatenate(arrays, axis=along)
    result, at, done = (lax.all_gather(both, axis, axis=dim, tiled=True), 0, [])
    for a in arrays:
        done.append(lax.slice_in_dim(result, at, at + a.shape[along], axis=along))
        at += a.shape[along]
    return tuple(done)


def laid_out(blocks, dim):
    blocks = jnp.moveaxis(blocks, 0, dim)
    lengths = blocks.shape
    return blocks.reshape(*lengths[:dim], lengths[dim] * lengths[dim + 1], *lengths[dim + 2 :])


def from_everyone(shard, axis):
    devices = lax.axis_size(axis)
    return lax.all_to_all(
        jnp.broadcast_to(shard[None], (devices, *shard.shape)), axis, 0, 0, tiled=True
    )


def gathered_copies(shard, axis, dim):
    return laid_out(from_everyone(shard, axis), dim)


def over_copies(shard, axis):
    return from_everyone(shard, axis).astype(jnp.float32).sum(axis=0)


def split_up(shard, dim, devices):
    lengths = shard.shape
    blocks = shard.reshape(*lengths[:dim], devices, lengths[dim] // devices, *lengths[dim + 1 :])
    return jnp.moveaxis(blocks, dim, 0)


def summed_on_arrival(shard, axis, dim):
    blocks = split_up(shard, dim, lax.axis_size(axis))
    arrived = lax.all_to_all(blocks, axis, split_axis=0, concat_axis=0, tiled=True)
    return arrived.astype(jnp.float32).sum(axis=0)


def of_everyone(shard, axis):
    everything = from_everyone(shard, axis)
    return jnp.sum(everything, axis=0)


def together(arrays, axis):
    ravelled, at, done = (jnp.concatenate([a.reshape(-1) for a in arrays]), 0, [])
    subtotal = of_everyone(ravelled, axis)
    for a in arrays:
        done.append(subtotal[at : at + a.size].reshape(a.shape))
        at += a.size
    return tuple(done)


def layer_norm(values, gain):
    mean = jnp.mean(values, axis=-1, keepdims=True)
    spread = jnp.mean(jnp.square(values - mean), axis=-1, keepdims=True)
    return (values - mean) * lax.rsqrt(spread + EPS) * gain


def body(
    tokens,
    lengths,
    cache_keys,
    cache_values,
    w_query,
    w_key,
    w_value,
    mix_weight,
    head_gain,
    w_out,
    first_gain,
    routing,
    route_weights,
    expert_gate,
    expert_up,
    expert_down,
    dense_gate,
    dense_up,
    dense_down,
    switch_vector,
    final_gain,
):
    f32 = jnp.float32
    bf16 = jnp.bfloat16
    seqs = tokens.shape[0]
    heads = mix_weight.shape[0]
    groups = cache_keys.shape[1]
    rep = heads // groups
    width = tokens.shape[1]
    pieces = in_one_piece((w_query, w_key, w_value), "ep", 0, 1)
    picked = tokens
    query32, key32, value32 = tuple(
        (jnp.dot(picked, piece, preferred_element_type=f32) for piece in pieces)
    )
    query = query32.astype(bf16).reshape(seqs, groups, rep, 2, HEAD)
    key_new = key32.astype(bf16).reshape(seqs, groups, 2, HEAD)
    value_new = value32.astype(bf16).reshape(seqs, groups, QK)
    keys = cache_keys.reshape(seqs, groups, cache_keys.shape[2], 2, HEAD)
    scale = HEAD ** (-0.5)
    cached = jnp.einsum("bgrmd,bglmd->bmgrl", query, keys, preferred_element_type=f32) * scale
    own = jnp.einsum("bgrmd,bgmd->bmgr", query, key_new, preferred_element_type=f32) * scale
    positions = lax.broadcasted_iota(jnp.int32, (1, cache_keys.shape[2]), 1)
    valid = (positions < lengths[:, None])[:, None, None, None, :]
    cached = jnp.where(valid, cached, -jnp.inf)
    top = jnp.maximum(jnp.max(cached, axis=-1), own)
    cached_exp = jnp.exp(cached - top[..., None])
    own_exp = jnp.exp(own - top)
    total = jnp.sum(cached_exp, axis=-1) + own_exp
    lam = mix_weight.reshape(groups, rep)
    mix_cached = (
        cached_exp[:, 0] / total[:, 0][..., None]
        - lam[None, :, :, None] * cached_exp[:, 1] / total[:, 1][..., None]
    ).astype(bf16)
    mix_own = (own_exp[:, 0] / total[:, 0] - lam[None] * own_exp[:, 1] / total[:, 1]).astype(bf16)
    head_out = jnp.einsum("bgrl,bgld->bgrd", mix_cached, cache_values, preferred_element_type=f32)
    head_out = head_out + mix_own.astype(f32)[..., None] * value_new.astype(f32)[:, :, None, :]
    square = jnp.mean(jnp.square(head_out), axis=-1, keepdims=True)
    normed = (head_out * lax.rsqrt(square + EPS) * head_gain).astype(bf16).reshape(seqs, heads * QK)
    group_part = jnp.dot(
        normed, gathered_copies(w_out, "ep", 1), preferred_element_type=f32
    ).astype(bf16)
    attention = over_copies(group_part.astype(f32).astype(jnp.bfloat16), "tp").astype(jnp.float32)
    hidden_state = layer_norm(tokens.astype(f32) + attention, first_gain).astype(bf16)
    experts = lax.axis_size("ep") // SPAN
    capacity = min(seqs, max(2, 2 * seqs * TOP // experts))
    quarter = width // lax.axis_size("tp")
    offset = lax.axis_index("tp") * quarter
    own_slice = lax.dynamic_slice_in_dim(hidden_state, offset, quarter, 1)
    flat_route = routing.reshape(-1)
    chosen = (flat_route[:, None] == jnp.arange(experts, dtype=jnp.int32)[None, :]).astype(
        jnp.int32
    )
    slot_rank = jnp.sum((jnp.cumsum(chosen, axis=0) - 1) * chosen, axis=1)
    slot_hit = (slot_rank[:, None] == jnp.arange(capacity, dtype=jnp.int32)[None, :]).astype(
        jnp.int32
    )
    placing = chosen[:, :, None] * slot_hit[:, None, :]
    repeated = jnp.repeat(hidden_state, TOP, axis=0)
    packed = jnp.einsum(
        "rec,rd->ecd", placing.astype(bf16), repeated, preferred_element_type=f32
    ).astype(bf16)
    cols = packed.shape[-1]
    arrived = lax.all_to_all(
        jnp.broadcast_to(packed[:, None], (experts, SPAN, capacity, cols)).reshape(
            experts * SPAN, capacity, cols
        ),
        "ep",
        split_axis=0,
        concat_axis=0,
        tiled=True,
    )
    slots = arrived.shape[1]
    rows = arrived.reshape(-1, width)
    gate = jnp.dot(rows, expert_gate[0], preferred_element_type=f32)
    lift = jnp.dot(rows, expert_up[0], preferred_element_type=f32)
    local_hidden = (jax.nn.silu(gate) * lift).astype(bf16)
    full_hidden = gathered_copies(local_hidden, "tp", 1)
    block_out = jnp.dot(full_hidden, expert_down[0], preferred_element_type=f32).astype(bf16)
    block_out = block_out.reshape(arrived.shape[0], slots, block_out.shape[-1])
    returned = lax.all_to_all(block_out, "ep", split_axis=0, concat_axis=0, tiled=True)
    per_expert = jnp.sum(returned.astype(f32).reshape(experts, SPAN, capacity, quarter), axis=1)
    weighting = placing.astype(f32) * route_weights.reshape(-1)[:, None, None]
    routed = jnp.einsum("rec,ecd->rd", weighting, per_expert, precision=lax.Precision.HIGHEST)
    routed = jnp.sum(routed.reshape(seqs, TOP, quarter), axis=1)
    piece = gathered_copies(own_slice, "ep", 0)
    gate_part = jnp.dot(piece, dense_gate, preferred_element_type=f32)
    up_part = jnp.dot(piece, dense_up, preferred_element_type=f32)
    pre_gate, pre_up = (
        over_copies(gate_part.astype(jnp.bfloat16), "tp").astype(jnp.float32),
        over_copies(up_part.astype(jnp.bfloat16), "tp").astype(jnp.float32),
    )
    dense_hidden = (jax.nn.silu(pre_gate) * pre_up).astype(bf16)
    picked = dense_hidden
    dense_out = summed_on_arrival(
        jnp.dot(picked, dense_down, preferred_element_type=f32).astype(jnp.bfloat16), "ep", 0
    ).astype(bf16)
    switch = jax.nn.sigmoid(jnp.sum(hidden_state.astype(f32) * switch_vector, axis=-1))
    combined = own_slice.astype(f32) + routed + switch[:, None] * dense_out.astype(f32)
    sums, squares = together(
        (jnp.sum(combined, axis=-1), jnp.sum(combined * combined, axis=-1)), "tp"
    )
    mean = sums / width
    spread = squares / width - mean * mean
    result = (combined - mean[:, None]) * lax.rsqrt(spread[:, None] + EPS) * final_gain
    return result.astype(bf16)


def solution(mesh):
    placed = (
        P("ep", None),
        P("ep"),
        P("ep", "tp", None, None),
        P("ep", "tp", None, None),
        P("ep", "tp"),
        P("ep", "tp"),
        P("ep", "tp"),
        P("tp"),
        P(),
        P("tp", "ep"),
        P(),
        P("ep", None),
        P("ep", None),
        P("ep", None, "tp"),
        P("ep", None, "tp"),
        P("ep", None, "tp"),
        P("tp", "ep"),
        P("tp", "ep"),
        P("ep", "tp"),
        P(),
        P("tp"),
    )
    return jax.shard_map(body, mesh=mesh, in_specs=placed, out_specs=P("ep", "tp"), check_vma=False)
```

profile of v0, /device:TPU:1, one launch (start us, length us, event | category | flops | bytes accessed | tf_op | source)
XLA Modules:
  0.0 253.8 jit_solution(8340567404205269793)
XLA Ops:
  8.1 2.4 broadcast_in_dim.32
  10.5 13.2 %all-to-all-start = ((bf16[64,512,32]{1,2,0:T(8,128)(2,1)}), bf16[64,512,32]{1,2,0:T(8,128)(2,1)}, u32[]{:S(2)}, u32[]{:S(2)}) async-start(bf16[64,512,32]{1,2,0:T(8,128)(2,1)} %broadcast_in_dim.32), calls=%async_computation | async-start | bytes 4194304 | tf_op jit(solution)/shard_map/all_to_all | solution.py:32
  23.7 4.0 %copy.87 = bf16[8,1,1024,128]{2,3,0,1:T(8,128)(2,1)} copy(bf16[8,1,1024,128]{3,2,1,0:T(8,128)(2,1)} %param.23) | data formatting | bytes 4194304 | tf_op args[2]
  27.8 66.9 %all-gather.2.cloned.1.call-done = bf16[2048,768]{1,0:T(8,128)(2,1)} async-done(((bf16[32,768]{1,0:T(8,128)(2,1)}), bf16[2048,768]{1,0:T(8,128)(2,1)}) %all-gather.2.cloned.1.call-update) | async-done | bytes 3145744 | tf_op jit(solution)/shard_map/all_gather | solution.py:17
  98.1 2.1 fusion.75
  102.9 2.2 convolution_convert_fusion.1
  105.8 4.4 %all-to-all-start.1 = ((bf16[4,8,2048]{2,1,0:T(8,128)(2,1)}), bf16[4,8,2048]{2,1,0:T(8,128)(2,1)S(1)}, u32[]{:S(2)}, u32[]{:S(2)}) async-start(bf16[4,8,2048]{2,1,0:T(8,128)(2,1)} %broadcast_in_dim.33), calls=%async_computation.1 | async-start | bytes 262144 | tf_op jit(solution)/shard_map/all_to_all | solution.py:32
  110.2 4.8 %all-to-all-done.1 = bf16[4,8,2048]{2,1,0:T(8,128)(2,1)S(1)} async-done(((bf16[4,8,2048]{2,1,0:T(8,128)(2,1)}), bf16[4,8,2048]{2,1,0:T(8,128)(2,1)S(1)}, u32[]{:S(2)}, u32[]{:S(2)}) %all-to-all-start.1) | async-done | bytes 131104 | tf_op jit(solution)/shard_map/all_to_all | solution.py:32
  116.5 8.4 %all-to-all-start.5 = ((bf16[64,8,512]{2,1,0:T(8,128)(2,1)}), bf16[64,8,512]{2,1,0:T(8,128)(2,1)S(1)}, u32[]{:S(2)}, u32[]{:S(2)}) async-start(bf16[64,8,512]{2,1,0:T(8,128)(2,1)} %broadcast_in_dim.37), calls=%async_computation.5 | async-start | bytes 1048576 | tf_op jit(solution)/shard_map/all_to_all | solution.py:32
  125.9 16.8 %all-to-all-done.5 = bf16[64,8,512]{2,1,0:T(8,128)(2,1)S(1)} async-done(((bf16[64,8,512]{2,1,0:T(8,128)(2,1)}), bf16[64,8,512]{2,1,0:T(8,128)(2,1)S(1)}, u32[]{:S(2)}, u32[]{:S(2)}) %all-to-all-start.5) | async-done | bytes 524320 | tf_op jit(solution)/shard_map/all_to_all | solution.py:32
  143.7 5.7 %all-to-all-start.2 = ((bf16[64,2,2048]{2,1,0:T(2,128)(2,1)}), bf16[64,2,2048]{2,1,0:T(2,128)(2,1)S(1)}, u32[]{:S(2)}, u32[]{:S(2)}) async-start(bf16[64,2,2048]{2,1,0:T(2,128)(2,1)} %bitcast.18), calls=%async_computation.2 | async-start | bytes 1048576 | tf_op jit(solution)/shard_map/all_to_all | solution.py:160
  149.7 17.4 %all-to-all-done.2 = bf16[64,2,2048]{2,1,0:T(2,128)(2,1)S(1)} async-done(((bf16[64,2,2048]{2,1,0:T(2,128)(2,1)}), bf16[64,2,2048]{2,1,0:T(2,128)(2,1)S(1)}, u32[]{:S(2)}, u32[]{:S(2)}) %all-to-all-start.2) | async-done | bytes 524320 | tf_op jit(solution)/shard_map/all_to_all | solution.py:160
  167.8 3.4 %all-to-all-start.6 = ((bf16[4,512,64]{1,2,0:T(8,128)(2,1)}), bf16[4,512,64]{1,2,0:T(8,128)(2,1)S(1)}, u32[]{:S(2)}, u32[]{:S(2)}) async-start(bf16[4,512,64]{1,2,0:T(8,128)(2,1)} %broadcast_in_dim.38), calls=%async_computation.6 | async-start | bytes 524288 | tf_op jit(solution)/shard_map/all_to_all | solution.py:32
  172.2 2.2 fusion.8
  175.0 2.3 all-to-all-done.6
  178.1 3.5 %all-to-all-start.3 = ((bf16[4,128,352]{1,2,0:T(8,128)(2,1)}), bf16[4,128,352]{1,2,0:T(8,128)(2,1)S(1)}, u32[]{:S(2)}, u32[]{:S(2)}) async-start(bf16[4,128,352]{1,2,0:T(8,128)(2,1)} %broadcast_in_dim.36), calls=%async_computation.3 | async-start | bytes 720896 | tf_op jit(solution)/shard_map/all_to_all | solution.py:32
  181.9 5.7 %all-to-all-done.3 = bf16[4,128,352]{1,2,0:T(8,128)(2,1)S(1)} async-done(((bf16[4,128,352]{1,2,0:T(8,128)(2,1)}), bf16[4,128,352]{1,2,0:T(8,128)(2,1)S(1)}, u32[]{:S(2)}, u32[]{:S(2)}) %all-to-all-start.3) | async-done | bytes 360480 | tf_op jit(solution)/shard_map/all_to_all | solution.py:32
  188.3 3.4 %all-to-all-start.7 = ((bf16[4,512,64]{1,2,0:T(8,128)(2,1)}), bf16[4,512,64]{1,2,0:T(8,128)(2,1)S(1)}, u32[]{:S(2)}, u32[]{:S(2)}) async-start(bf16[4,512,64]{1,2,0:T(8,128)(2,1)} %broadcast_in_dim.39), calls=%async_computation.7 | async-start | bytes 524288 | tf_op jit(solution)/shard_map/all_to_all | solution.py:32
  194.2 3.0 %all-to-all-done.7 = bf16[4,512,64]{1,2,0:T(8,128)(2,1)S(1)} async-done(((bf16[4,512,64]{1,2,0:T(8,128)(2,1)}), bf16[4,512,64]{1,2,0:T(8,128)(2,1)S(1)}, u32[]{:S(2)}, u32[]{:S(2)}) %all-to-all-start.7) | async-done | bytes 262176 | tf_op jit(solution)/shard_map/all_to_all | solution.py:32
  197.2 8.8 %all-to-all-start.4 = ((bf16[64,2,512]{2,1,0:T(2,128)(2,1)}), bf16[64,2,512]{2,1,0:T(2,128)(2,1)S(1)}, u32[]{:S(2)}, u32[]{:S(2)}) async-start(bf16[64,2,512]{2,1,0:T(2,128)(2,1)} %reshape.305), calls=%async_computation.4 | async-start | bytes 262144 | tf_op jit(solution)/shard_map/all_to_all | solution.py:177
  207.1 9.9 %all-to-all-done.4 = bf16[64,2,512]{2,1,0:T(2,128)(2,1)S(1)} async-done(((bf16[64,2,512]{2,1,0:T(2,128)(2,1)}), bf16[64,2,512]{2,1,0:T(2,128)(2,1)S(1)}, u32[]{:S(2)}, u32[]{:S(2)}) %all-to-all-start.4) | async-done | bytes 131104 | tf_op jit(solution)/shard_map/all_to_all | solution.py:177
  217.1 4.5 %all-to-all-start.8 = ((bf16[64,8,512]{2,1,0:T(8,128)(2,1)}), bf16[64,8,512]{2,1,0:T(8,128)(2,1)S(1)}, u32[]{:S(2)}, u32[]{:S(2)}) async-start(bf16[64,8,512]{2,1,0:T(8,128)(2,1)} %fusion.10), calls=%async_computation.8 | async-start | bytes 1048576 | tf_op jit(solution)/shard_map/all_to_all | solution.py:53
  222.2 17.1 %all-to-all-done.8 = bf16[64,8,512]{2,1,0:T(8,128)(2,1)S(1)} async-done(((bf16[64,8,512]{2,1,0:T(8,128)(2,1)}), bf16[64,8,512]{2,1,0:T(8,128)(2,1)S(1)}, u32[]{:S(2)}, u32[]{:S(2)}) %all-to-all-start.8) | async-done | bytes 524320 | tf_op jit(solution)/shard_map/all_to_all | solution.py:53
  239.7 6.5 %all_to_all.51 = f32[4,1,16]{2,1,0:T(1,128)S(1)} all-to-all(f32[4,1,16]{2,1,0:T(1,128)S(1)} %broadcast_in_dim.40), channel_id=1, replica_groups=mesh['ep'=64,'tp'=4] {'tp'}, dimensions={0} | all-to-all | bytes 512 | tf_op jit(solution)/shard_map/all_to_all | solution.py:32
  (101 shorter events, 21.7 us)
Async XLA Ops:
  6.5 95.7 %copy-start = (bf16[8,1,1024,128]{3,2,1,0:T(8,128)(2,1)S(1)}, bf16[8,1,1024,128]{3,2,1,0:T(8,128)(2,1)}, u32[]{:S(2)}) copy-start(bf16[8,1,1024,128]{3,2,1,0:T(8,128)(2,1)} %param.24) | copy-start | bytes 6291460
  6.5 88.1 %all-gather.2.cloned.1.call-start = ((), (), s32[]{:S(2)}) async-start(), calls=%async_computation.10 | async-start | bytes 3194880 | tf_op jit(solution)/shard_map/all_gather | solution.py:17
  10.5 92.4 %all-to-all-start = ((bf16[64,512,32]{1,2,0:T(8,128)(2,1)}), bf16[64,512,32]{1,2,0:T(8,128)(2,1)}, u32[]{:S(2)}, u32[]{:S(2)}) async-start(bf16[64,512,32]{1,2,0:T(8,128)(2,1)} %broadcast_in_dim.32), calls=%async_computation | async-start | bytes 4194304 | tf_op jit(solution)/shard_map/all_to_all | solution.py:32
  23.7 4.0 %copy-start.11 = (s32[8]{0:T(128)S(1)}, s32[8]{0:T(128)}, u32[]{:S(2)}) copy-start(s32[8]{0:T(128)} %param.22) | copy-start | bytes 100
  23.7 71.0 %copy-start.2 = (bf16[8,2048]{1,0:T(8,128)(2,1)S(1)}, bf16[8,2048]{1,0:T(8,128)(2,1)}, u32[]{:S(2)}) copy-start(bf16[8,2048]{1,0:T(8,128)(2,1)} %param.21) | copy-start | bytes 98308
  97.9 2.9 %copy-start.12 = (f32[4]{0:T(128)S(1)}, f32[4]{0:T(128)}, u32[]{:S(2)}) copy-start(f32[4]{0:T(128)} %param.28) | copy-start | bytes 52
  100.5 2.3 copy-start.10
  102.8 12.7 %copy-start.6 = (f32[2048]{0:T(1024)S(1)}, f32[2048]{0:T(1024)}, u32[]{:S(2)}) copy-start(f32[2048]{0:T(1024)} %param.40) | copy-start | bytes 24580
  102.8 12.7 %copy-start.7 = (f32[2048]{0:T(1024)S(1)}, f32[2048]{0:T(1024)}, u32[]{:S(2)}) copy-start(f32[2048]{0:T(1024)} %param.31) | copy-start | bytes 24580
  102.9 22.0 %copy-start.8 = (s32[8,2]{0,1:T(2,128)S(1)}, s32[8,2]{0,1:T(2,128)}, u32[]{:S(2)}) copy-start(s32[8,2]{0,1:T(2,128)} %param.32) | copy-start | bytes 196
  105.8 9.3 %all-to-all-start.1 = ((bf16[4,8,2048]{2,1,0:T(8,128)(2,1)}), bf16[4,8,2048]{2,1,0:T(8,128)(2,1)S(1)}, u32[]{:S(2)}, u32[]{:S(2)}) async-start(bf16[4,8,2048]{2,1,0:T(8,128)(2,1)} %broadcast_in_dim.33), calls=%async_computation.1 | async-start | bytes 262144 | tf_op jit(solution)/shard_map/all_to_all | solution.py:32
  115.5 34.0 %copy-start.3 = (bf16[512,64]{0,1:T(8,128)(2,1)S(1)}, bf16[512,64]{0,1:T(8,128)(2,1)}, u32[]{:S(2)}) copy-start(bf16[512,64]{0,1:T(8,128)(2,1)} %param.37) | copy-start | bytes 196612
  116.5 26.1 %all-to-all-start.5 = ((bf16[64,8,512]{2,1,0:T(8,128)(2,1)}), bf16[64,8,512]{2,1,0:T(8,128)(2,1)S(1)}, u32[]{:S(2)}, u32[]{:S(2)}) async-start(bf16[64,8,512]{2,1,0:T(8,128)(2,1)} %broadcast_in_dim.37), calls=%async_computation.5 | async-start | bytes 1048576 | tf_op jit(solution)/shard_map/all_to_all | solution.py:32
  143.7 23.4 %all-to-all-start.2 = ((bf16[64,2,2048]{2,1,0:T(2,128)(2,1)}), bf16[64,2,2048]{2,1,0:T(2,128)(2,1)S(1)}, u32[]{:S(2)}, u32[]{:S(2)}) async-start(bf16[64,2,2048]{2,1,0:T(2,128)(2,1)} %bitcast.18), calls=%async_computation.2 | async-start | bytes 1048576 | tf_op jit(solution)/shard_map/all_to_all | solution.py:160
  167.8 9.5 %all-to-all-start.6 = ((bf16[4,512,64]{1,2,0:T(8,128)(2,1)}), bf16[4,512,64]{1,2,0:T(8,128)(2,1)S(1)}, u32[]{:S(2)}, u32[]{:S(2)}) async-start(bf16[4,512,64]{1,2,0:T(8,128)(2,1)} %broadcast_in_dim.38), calls=%async_computation.6 | async-start | bytes 524288 | tf_op jit(solution)/shard_map/all_to_all | solution.py:32
  172.2 2.2 copy-start.13
  174.5 7.1 %copy-start.4 = (bf16[512,64]{0,1:T(8,128)(2,1)S(1)}, bf16[512,64]{0,1:T(8,128)(2,1)}, u32[]{:S(2)}) copy-start(bf16[512,64]{0,1:T(8,128)(2,1)} %param.38) | copy-start | bytes 196612
  178.1 9.5 %all-to-all-start.3 = ((bf16[4,128,352]{1,2,0:T(8,128)(2,1)}), bf16[4,128,352]{1,2,0:T(8,128)(2,1)S(1)}, u32[]{:S(2)}, u32[]{:S(2)}) async-start(bf16[4,128,352]{1,2,0:T(8,128)(2,1)} %broadcast_in_dim.36), calls=%async_computation.3 | async-start | bytes 720896 | tf_op jit(solution)/shard_map/all_to_all | solution.py:32
  181.8 24.2 %copy-start.5 = (bf16[64,512]{1,0:T(8,128)(2,1)S(1)}, bf16[64,512]{1,0:T(8,128)(2,1)}, u32[]{:S(2)}) copy-start(bf16[64,512]{1,0:T(8,128)(2,1)} %param.39) | copy-start | bytes 196612
  188.3 8.9 %all-to-all-start.7 = ((bf16[4,512,64]{1,2,0:T(8,128)(2,1)}), bf16[4,512,64]{1,2,0:T(8,128)(2,1)S(1)}, u32[]{:S(2)}, u32[]{:S(2)}) async-start(bf16[4,512,64]{1,2,0:T(8,128)(2,1)} %broadcast_in_dim.39), calls=%async_computation.7 | async-start | bytes 524288 | tf_op jit(solution)/shard_map/all_to_all | solution.py:32
  191.7 30.2 %copy-start.14 = (f32[8,2]{0,1:T(2,128)S(1)}, f32[8,2]{0,1:T(2,128)}, u32[]{:S(2)}) copy-start(f32[8,2]{0,1:T(2,128)} %param.33) | copy-start | bytes 196
  193.5 52.8 %copy-start.9 = (f32[512]{0:T(512)S(1)}, f32[512]{0:T(512)}, u32[]{:S(2)}) copy-start(f32[512]{0:T(512)} %param.41) | copy-start | bytes 6148
  197.2 19.9 %all-to-all-start.4 = ((bf16[64,2,512]{2,1,0:T(2,128)(2,1)}), bf16[64,2,512]{2,1,0:T(2,128)(2,1)S(1)}, u32[]{:S(2)}, u32[]{:S(2)}) async-start(bf16[64,2,512]{2,1,0:T(2,128)(2,1)} %reshape.305), calls=%async_computation.4 | async-start | bytes 262144 | tf_op jit(solution)/shard_map/all_to_all | solution.py:177
  217.1 22.3 %all-to-all-start.8 = ((bf16[64,8,512]{2,1,0:T(8,128)(2,1)}), bf16[64,8,512]{2,1,0:T(8,128)(2,1)S(1)}, u32[]{:S(2)}, u32[]{:S(2)}) async-start(bf16[64,8,512]{2,1,0:T(8,128)(2,1)} %fusion.10), calls=%async_computation.8 | async-start | bytes 1048576 | tf_op jit(solution)/shard_map/all_to_all | solution.py:53
  (1 other events, 2.2 us)
Sparse Core Ops, SparseCore 0:
  10.1 84.4 all-gather.1
where the time goes:
time: 255 us; the launch traced here: 254 us
  waiting for transfers between devices  144 us (56%)
  starting transfers between devices  55.2 us (22%)
  matrix products  16 us (6%)
  local copies, waits for them, and re-layouts  14.2 us (6%)
  between operations  13.7 us (5%)
  blocking collectives  6.46 us (3%)
  other arithmetic  4.36 us (2%)
    all_gather x1, waiting for transfers between devices, in_one_piece(): result, at, done = (lax.all_gather(both, axis, axis=dim, tiled=True), 0, [])  66.9 us
    all_to_all x6, starting transfers between devices, from_everyone(): lax.all_to_all(jnp.broadcast_to(shard[None], (devices, *shard.shape)), ax...  36.3 us
    all_to_all x6, waiting for transfers between devices, from_everyone(): lax.all_to_all(jnp.broadcast_to(shard[None], (devices, *shard.shape)), ax...  32.5 us
    all_to_all x1, waiting for transfers between devices, body(): lax.all_to_all(jnp.broadcast_to(packed[:, None], (experts, SPAN, capacity...  17.4 us
    all_to_all x1, waiting for transfers between devices, summed_on_arrival(): lax.all_to_all(blocks, axis, split_axis=0, concat_axis=0, tiled=True)  17.1 us
    all_to_all x1, waiting for transfers between devices, body(): lax.all_to_all(block_out, 'ep', split_axis=0, concat_axis=0, tiled=True)  9.91 us
    all_to_all x1, starting transfers between devices, body(): lax.all_to_all(block_out, 'ep', split_axis=0, concat_axis=0, tiled=True)  8.76 us
    all_to_all x1, blocking collectives, from_everyone(): lax.all_to_all(jnp.broadcast_to(shard[None], (devices, *shard.shape)), ax...  6.46 us
  transfers between devices with their start and end apart: 10, of which 9 were waited for; matrix products, arithmetic and copies ran while one was open for 10% of the time, Pallas kernels for 0%

commit v1 on v0

--- a/solution.py
+++ b/solution.py
@@ -1,6 +1,10 @@
+from types import SimpleNamespace
+
 import jax
 import jax.numpy as jnp
 from jax import lax
+from jax.experimental import pallas as pl
+from jax.experimental.pallas import tpu as pltpu
 from jax.sharding import PartitionSpec as P
 
 QK = 128
@@ -10,6 +14,273 @@
 
 
 EPS = 1e-05
+
+
+NZ, NQ, NT = 8, 8, 4
+MESH_ID = pl.DeviceIdType.MESH
+F32 = jnp.float32
+BF16 = jnp.bfloat16
+NT_DIMS = (((1,), (1,)), ((), ()))
+
+
+def dot(a, b):
+    return jnp.dot(a, b, preferred_element_type=F32)
+
+
+def dot_nt(a, b):
+    return lax.dot_general(a, b, NT_DIMS, preferred_element_type=F32)
+
+
+def eye(n):
+    r = lax.broadcasted_iota(jnp.int32, (n, n), 0)
+    c = lax.broadcasted_iota(jnp.int32, (n, n), 1)
+    return jnp.where(r == c, 1.0, 0.0).astype(BF16)
+
+
+def stacked(ref, n):
+    return jnp.concatenate([ref[i].astype(F32) for i in range(n)], axis=0).astype(BF16)
+
+
+A_SCRATCH = dict(
+    tok_v=pltpu.VMEM((8, 2048), BF16),
+    tokg=pltpu.VMEM((NZ, 8, 256), BF16),
+    wg=pltpu.VMEM((256, 768), BF16),
+    wo_raw=pltpu.VMEM((512, 32), BF16),
+    wog=pltpu.VMEM((256, 512), BF16),
+    kbuf=pltpu.VMEM((8, 1024, 128), BF16),
+    vbuf=pltpu.VMEM((8, 1024, 128), BF16),
+    fg_v=pltpu.VMEM((1, 2048), F32),
+    hg_v=pltpu.VMEM((1, 128), F32),
+    pbuf=pltpu.VMEM((NZ, 8, 768), F32),
+    precv=pltpu.VMEM((NZ, 8, 768), F32),
+    qv=pltpu.VMEM((8, 768), F32),
+    qs=pltpu.VMEM((8, 8, 128), F32),
+    nv=pltpu.VMEM((8, 512), F32),
+    ng=pltpu.VMEM((NQ, 8, 512), BF16),
+    gbuf=pltpu.VMEM((NQ, 8, 256), BF16),
+    attr=pltpu.VMEM((NT, NQ, 8, 256), BF16),
+    lsem=pltpu.SemaphoreType.DMA((10,)),
+    s_wg=pltpu.SemaphoreType.DMA((NQ,)),
+    r_wg=pltpu.SemaphoreType.DMA((NQ,)),
+    s_tok=pltpu.SemaphoreType.DMA((NZ,)),
+    r_tok=pltpu.SemaphoreType.DMA((NZ,)),
+    s_wo=pltpu.SemaphoreType.DMA((NZ,)),
+    r_wo=pltpu.SemaphoreType.DMA((NZ,)),
+    s_p=pltpu.SemaphoreType.DMA((NZ,)),
+    r_p=pltpu.SemaphoreType.DMA((NZ,)),
+    s_n=pltpu.SemaphoreType.DMA((NQ,)),
+    r_n=pltpu.SemaphoreType.DMA((NQ,)),
+    s_a=pltpu.SemaphoreType.DMA((NT * NQ,)),
+    r_a=pltpu.SemaphoreType.DMA((NT * NQ,)),
+)
+
+
+def remote(src, dst, send, recv, ep, tp):
+    return pltpu.make_async_remote_copy(
+        src_ref=src, dst_ref=dst, send_sem=send, recv_sem=recv,
+        device_id=(ep, tp), device_id_type=MESH_ID,
+    )
+
+
+def where_am_i():
+    ep, tp = lax.axis_index("ep"), lax.axis_index("tp")
+    return ep // NQ, lax.rem(ep, NQ), tp
+
+
+def attention_kernel(
+    lengths, mixw, tokens, keys, values, wq, wk, wv, wout, hgain, fgain, out, *scratch
+):
+    s = SimpleNamespace(**dict(zip(A_SCRATCH, scratch)))
+    z, q, y = where_am_i()
+    me = z * NQ + q
+
+    qrow = pl.multiple_of(q * 32, 32)
+    zrow = pl.multiple_of(z * 32, 32)
+    first = [
+        pltpu.make_async_copy(tokens, s.tok_v, s.lsem.at[0]),
+        pltpu.make_async_copy(wq, s.wg.at[pl.ds(qrow, 32), pl.ds(0, 512)], s.lsem.at[1]),
+        pltpu.make_async_copy(wk, s.wg.at[pl.ds(qrow, 32), pl.ds(512, 128)], s.lsem.at[2]),
+        pltpu.make_async_copy(wv, s.wg.at[pl.ds(qrow, 32), pl.ds(640, 128)], s.lsem.at[3]),
+        pltpu.make_async_copy(wout, s.wo_raw, s.lsem.at[4]),
+    ]
+    later = [
+        pltpu.make_async_copy(keys, s.kbuf, s.lsem.at[5]),
+        pltpu.make_async_copy(values, s.vbuf, s.lsem.at[6]),
+        pltpu.make_async_copy(fgain, s.fg_v, s.lsem.at[7]),
+        pltpu.make_async_copy(hgain, s.hg_v, s.lsem.at[8]),
+    ]
+    for c in first:
+        c.start()
+
+    barrier = pltpu.get_barrier_semaphore()
+    for d in range(1, NZ):
+        pl.semaphore_signal(
+            barrier, inc=1, device_id=(lax.rem(z + d, NZ) * NQ + q, y), device_id_type=MESH_ID
+        )
+    for dy in range(NT):
+        for dq in range(NQ):
+            if dy or dq:
+                pl.semaphore_signal(
+                    barrier, inc=1,
+                    device_id=(z * NQ + lax.rem(q + dq, NQ), lax.rem(y + dy, NT)),
+                    device_id_type=MESH_ID,
+                )
+    for c in later:
+        c.start()
+    first[4].wait()
+    s.wog[pl.ds(zrow, 32), :] = dot_nt(eye(32), s.wo_raw[...]).astype(BF16)
+    for c in first[:4]:
+        c.wait()
+    pl.semaphore_wait(barrier, NZ - 1 + NT * NQ - 1)
+
+    wg_copies, tok_copies, wo_copies = [], [], []
+    for d in range(1, NZ):
+        zz = lax.rem(z + d, NZ)
+        c = remote(
+            s.tok_v.at[:, pl.ds(pl.multiple_of(zz * 256, 256), 256)], s.tokg.at[z],
+            s.s_tok.at[d], s.r_tok.at[d], zz * NQ + q, y,
+        )
+        c.start()
+        tok_copies.append(c)
+    for d in range(1, NQ):
+        mine = s.wg.at[pl.ds(qrow, 32), :]
+        c = remote(mine, mine, s.s_wg.at[d], s.r_wg.at[d], z * NQ + lax.rem(q + d, NQ), y)
+        c.start()
+        wg_copies.append(c)
+    for d in range(1, NZ):
+        mine = s.wog.at[pl.ds(zrow, 32), :]
+        c = remote(mine, mine, s.s_wo.at[d], s.r_wo.at[d], lax.rem(z + d, NZ) * NQ + q, y)
+        c.start()
+        wo_copies.append(c)
+    s.tokg[z] = s.tok_v[:, pl.ds(pl.multiple_of(z * 256, 256), 256)]
+
+    for c in tok_copies + wg_copies:
+        c.wait_recv()
+    part = dot(stacked(s.tokg, NZ), s.wg[...])
+    for i in range(NZ):
+        s.pbuf[i] = part[i * 8:(i + 1) * 8]
+    p_copies = []
+    for d in range(1, NZ):
+        zz = lax.rem(z + d, NZ)
+        c = remote(s.pbuf.at[zz], s.precv.at[z], s.s_p.at[d], s.r_p.at[d], zz * NQ + q, y)
+        c.start()
+        p_copies.append(c)
+    s.precv[z] = s.pbuf[z]
+    for c in p_copies:
+        c.wait_recv()
+    total = s.precv[0]
+    for i in range(1, NZ):
+        total = total + s.precv[i]
+    s.qv[...] = total.astype(BF16).astype(F32)
+    for b in range(8):
+        for r in range(4):
+            row = s.qv[b:b + 1, r * 128:(r + 1) * 128]
+            s.qs[b, r:r + 1, :] = row
+            s.qs[b, r + 4:r + 5, :] = row
+
+    for c in later:
+        c.wait()
+    sub = lax.broadcasted_iota(jnp.int32, (8, 128), 0)
+    lane = lax.broadcasted_iota(jnp.int32, (8, 128), 1)
+    half = (sub >= 4) == (lane >= 64)
+    col = lax.broadcasted_iota(jnp.int32, (8, 1024), 1)
+    rows1 = lax.broadcasted_iota(jnp.int32, (8, 1), 0)
+    lam = jnp.zeros((8, 1), F32)
+    for r in range(4):
+        lam = jnp.where(rows1 == r + 4, mixw[r], lam)
+    weight = jnp.where(rows1 < 4, 1.0, -lam)
+    for b in range(8):
+        q8 = jnp.where(half, s.qs[b], 0.0)
+        knew = s.qv[b:b + 1, 512:640]
+        vnew = s.qv[b:b + 1, 640:768]
+        sc = dot_nt(q8.astype(BF16), s.kbuf[b]) * 0.125
+        own = jnp.sum(q8 * knew, axis=1, keepdims=True) * 0.125
+        sc = jnp.where(col < lengths[b], sc, -jnp.inf)
+        top = jnp.maximum(jnp.max(sc, axis=1, keepdims=True), own)
+        e = jnp.exp(sc - top)
+        eo = jnp.exp(own - top)
+        scale = weight / (jnp.sum(e, axis=1, keepdims=True) + eo)
+        t = e * scale
+        mix = (t + pltpu.roll(t, 4, 0)).astype(BF16)
+        to = jnp.broadcast_to(eo * scale, (8, 128))
+        mix_own = (to + pltpu.roll(to, 4, 0)).astype(BF16).astype(F32)
+        ho = dot(mix, s.vbuf[b]) + mix_own * vnew
+        square = jnp.mean(ho * ho, axis=1, keepdims=True)
+        n8 = ho * lax.rsqrt(square + EPS) * s.hg_v[...]
+        for r in range(4):
+            s.nv[b:b + 1, r * 128:(r + 1) * 128] = n8[r:r + 1, :]
+    s.ng[q] = s.nv[...].astype(BF16)
+    n_copies = []
+    for d in range(1, NQ):
+        c = remote(
+            s.ng.at[q], s.ng.at[q], s.s_n.at[d], s.r_n.at[d], z * NQ + lax.rem(q + d, NQ), y
+        )
+        c.start()
+        n_copies.append(c)
+    for c in wo_copies + n_copies:
+        c.wait_recv()
+    group = dot_nt(stacked(s.ng, NQ), s.wog[...])
+    for i in range(NQ):
+        s.gbuf[i] = group[i * 8:(i + 1) * 8].astype(BF16)
+    a_copies = []
+    for dy in range(NT):
+        for dq in range(NQ):
+            if dy or dq:
+                qq = lax.rem(q + dq, NQ)
+                c = remote(
+                    s.gbuf.at[qq], s.attr.at[y, q], s.s_a.at[dy * NQ + dq],
+                    s.r_a.at[dy * NQ + dq], z * NQ + qq, lax.rem(y + dy, NT),
+                )
+                c.start()
+                a_copies.append(c)
+    s.attr[y, q] = s.gbuf[q]
+    for c in a_copies:
+        c.wait_recv()
+    parts = []
+    for i in range(NQ):
+        acc = s.attr[0, i].astype(F32)
+        for t in range(1, NT):
+            acc = acc + s.attr[t, i].astype(F32)
+        parts.append(acc)
+    lane32 = lane // 32
+    tiles = []
+    for zz in range(NZ):
+        for h in range(2):
+            tile = None
+            for k in range(4):
+                off = zz * 32
+                piece = parts[h * 4 + k][:, (off // 128) * 128:(off // 128) * 128 + 128]
+                shift = (k * 32 - off % 128) % 128
+                if shift:
+                    piece = pltpu.roll(piece, shift, 1)
+                tile = piece if tile is None else jnp.where(lane32 == k, piece, tile)
+            tiles.append(tile)
+    x = s.tok_v[...].astype(F32) + jnp.concatenate(tiles, axis=1)
+    mean = jnp.mean(x, axis=1, keepdims=True)
+    xc = x - mean
+    spread = jnp.mean(xc * xc, axis=1, keepdims=True)
+    out[...] = (xc * lax.rsqrt(spread + EPS) * s.fg_v[...]).astype(BF16)
+    for c in tok_copies + wg_copies + wo_copies + p_copies + n_copies + a_copies:
+        c.wait_send()
+
+
+def attention(tokens, lengths, keys, values, wq, wk, wv, mixw, hgain, wout, fgain):
+    anywhere = pl.BlockSpec(memory_space=pl.ANY)
+    smem = pl.BlockSpec(memory_space=pltpu.SMEM)
+    return pl.pallas_call(
+        attention_kernel,
+        out_shape=jax.ShapeDtypeStruct((8, 2048), BF16),
+        in_specs=[smem, smem] + [anywhere] * 9,
+        out_specs=pl.BlockSpec(memory_space=pltpu.VMEM),
+        scratch_shapes=list(A_SCRATCH.values()),
+        compiler_params=pltpu.CompilerParams(
+            collective_id=0, has_side_effects=True, vmem_limit_bytes=40 * 1024 * 1024
+        ),
+        name="attention",
+    )(
+        lengths, mixw, tokens, keys.reshape(8, 1024, 128), values.reshape(8, 1024, 128),
+        wq, wk, wv, wout, hgain.reshape(1, 128), fgain.reshape(1, 2048),
+    )
 
 
 def in_one_piece(arrays, axis, dim, along):
@@ -104,40 +375,10 @@
     groups = cache_keys.shape[1]
     rep = heads // groups
     width = tokens.shape[1]
-    pieces = in_one_piece((w_query, w_key, w_value), "ep", 0, 1)
-    picked = tokens
-    query32, key32, value32 = tuple(
-        (jnp.dot(picked, piece, preferred_element_type=f32) for piece in pieces)
-    )
-    query = query32.astype(bf16).reshape(seqs, groups, rep, 2, HEAD)
-    key_new = key32.astype(bf16).reshape(seqs, groups, 2, HEAD)
-    value_new = value32.astype(bf16).reshape(seqs, groups, QK)
-    keys = cache_keys.reshape(seqs, groups, cache_keys.shape[2], 2, HEAD)
-    scale = HEAD ** (-0.5)
-    cached = jnp.einsum("bgrmd,bglmd->bmgrl", query, keys, preferred_element_type=f32) * scale
-    own = jnp.einsum("bgrmd,bgmd->bmgr", query, key_new, preferred_element_type=f32) * scale
-    positions = lax.broadcasted_iota(jnp.int32, (1, cache_keys.shape[2]), 1)
-    valid = (positions < lengths[:, None])[:, None, None, None, :]
-    cached = jnp.where(valid, cached, -jnp.inf)
-    top = jnp.maximum(jnp.max(cached, axis=-1), own)
-    cached_exp = jnp.exp(cached - top[..., None])
-    own_exp = jnp.exp(own - top)
-    total = jnp.sum(cached_exp, axis=-1) + own_exp
-    lam = mix_weight.reshape(groups, rep)
-    mix_cached = (
-        cached_exp[:, 0] / total[:, 0][..., None]
-        - lam[None, :, :, None] * cached_exp[:, 1] / total[:, 1][..., None]
-    ).astype(bf16)
-    mix_own = (own_exp[:, 0] / total[:, 0] - lam[None] * own_exp[:, 1] / total[:, 1]).astype(bf16)
-    head_out = jnp.einsum("bgrl,bgld->bgrd", mix_cached, cache_values, preferred_element_type=f32)
-    head_out = head_out + mix_own.astype(f32)[..., None] * value_new.astype(f32)[:, :, None, :]
-    square = jnp.mean(jnp.square(head_out), axis=-1, keepdims=True)
-    normed = (head_out * lax.rsqrt(square + EPS) * head_gain).astype(bf16).reshape(seqs, heads * QK)
-    group_part = jnp.dot(
-        normed, gathered_copies(w_out, "ep", 1), preferred_element_type=f32
-    ).astype(bf16)
-    attention = over_copies(group_part.astype(f32).astype(jnp.bfloat16), "tp").astype(jnp.float32)
-    hidden_state = layer_norm(tokens.astype(f32) + attention, first_gain).astype(bf16)
+    hidden_state = attention(
+        tokens, lengths, cache_keys, cache_values, w_query, w_key, w_value, mix_weight,
+        head_gain, w_out, first_gain,
+    )
     experts = lax.axis_size("ep") // SPAN
     capacity = min(seqs, max(2, 2 * seqs * TOP // experts))
     quarter = width // lax.axis_size("tp")

time: 255 us -> 179 us (0.70)
  waiting for transfers between devices: 144 us -> 74.3 us
  Pallas kernels: 0 us -> 39.9 us
  starting transfers between devices: 55.2 us -> 35 us
  between operations: 13.7 us -> 0.31 us
  matrix products: 16 us -> 5.1 us
    all_gather x1 -> x0, waiting for transfers between devices: 66.9 us -> none  [in_one_piece(): result, at, done = (lax.all_gather(both, axis, axis=dim, tiled=True), 0, [])]
    pallas_call x0 -> x1, Pallas kernels: none -> 39.9 us  [attention(): pl.pallas_call(attention_kernel, out_shape=jax.ShapeDtypeStruct((8, 2048)...]
    all_to_all x6 -> x4, starting transfers between devices: 36.3 us -> 16.1 us  [from_everyone(): lax.all_to_all(jnp.broadcast_to(shard[None], (devices, *shard.shape)), ax...]
    dot_general x7 -> x0, matrix products: 9.39 us -> none  [the longest x3 4.41 us: body(): jnp.dot(picked, piece, preferred_element_type=f32)]
    unnamed x32 -> x40, local copies, waits for them, and re-layouts: 4.16 us -> 9.87 us
    broadcast_in_dim x7 -> x5, local copies, waits for them, and re-layouts: 6.08 us -> 3.02 us  [from_everyone(): jnp.broadcast_to(shard[None], (devices, *shard.shape))]
    all_to_all x6 -> x4, waiting for transfers between devices: 32.5 us -> 30 us  [from_everyone(): lax.all_to_all(jnp.broadcast_to(shard[None], (devices, *shard.shape)), ax...]
  transfers between devices with their start and end apart: 10 -> 7, of which waited for: 9 -> 7; matrix products, arithmetic and copies ran while one was open for 10% -> 4% of each run, Pallas kernels for 0% -> 0%
where the time goes in v1:
time: 179 us; the launch traced here: 178 us
  waiting for transfers between devices  74.3 us (42%)
  Pallas kernels  39.9 us (22%)
  starting transfers between devices  35 us (20%)
  local copies, waits for them, and re-layouts  15.4 us (9%)
  blocking collectives  6.46 us (4%)
  matrix products  5.1 us (3%)
  other arithmetic  1.85 us (1%)
    pallas_call x1, Pallas kernels, attention(): pl.pallas_call(attention_kernel, out_shape=jax.ShapeDtypeStruct((8, 2048)...  39.9 us
    all_to_all x4, waiting for transfers between devices, from_everyone(): lax.all_to_all(jnp.broadcast_to(shard[None], (devices, *shard.shape)), ax...  30 us
    all_to_all x1, waiting for transfers between devices, body(): lax.all_to_all(jnp.broadcast_to(packed[:, None], (experts, SPAN, capacity...  17.2 us
    all_to_all x1, waiting for transfers between devices, summed_on_arrival(): lax.all_to_all(blocks, axis, split_axis=0, concat_axis=0, tiled=True)  17.1 us
    all_to_all x4, starting transfers between devices, from_everyone(): lax.all_to_all(jnp.broadcast_to(shard[None], (devices, *shard.shape)), ax...  16.1 us
    all_to_all x1, waiting for transfers between devices, body(): lax.all_to_all(block_out, 'ep', split_axis=0, concat_axis=0, tiled=True)  9.9 us
    unnamed x40, local copies, waits for them, and re-layouts  9.87 us
    all_to_all x1, starting transfers between devices, body(): lax.all_to_all(block_out, 'ep', split_axis=0, concat_axis=0, tiled=True)  8.76 us
  transfers between devices with their start and end apart: 7, of which 7 were waited for; matrix products, arithmetic and copies ran while one was open for 4% of the time, Pallas kernels for 0%

profile of v1, /device:TPU:1, one launch (start us, length us, event | category | flops | bytes accessed | tf_op | source)
XLA Modules:
  0.0 178.4 jit_solution(9528137323153580994)
XLA Ops:
  0.0 1.0 copy.53.wout
  1.0 1.6 copy-done.1
  2.6 1.6 copy-done.2
  9.8 39.9 %attention.1 = bf16[8,2048]{1,0:T(8,128)(2,1)S(1)} custom-call(s32[8]{0:T(128)S(1)} %copy-done.8, f32[4]{0:T(128)S(1)} %copy-done.9, bf16[8,2048]{1,0:T(8,128)(2,1)S(1)} %copy-done.3, bf16[8,1024,128]{2,1,0:T(8,128)(2,1)S(1)} %bitcast.49, bf16[8,1024,128]{2,1,0:T(8,128)(2,1)S(1)} %bitcast.50, bf16[32,512]{1,0:T(8,128)(2,1)S(1)} %copy-done.4, ...), custom_call_target="tpu_custom_call" | custom-call | tf_op jit(solution)/shard_map/attention/pallas_call | solution.py:270
  49.7 0.8 broadcast_in_dim.17
  50.6 5.8 %all-to-all-start.3 = ((bf16[64,8,512]{2,1,0:T(8,128)(2,1)}), bf16[64,8,512]{2,1,0:T(8,128)(2,1)S(1)}, u32[]{:S(2)}, u32[]{:S(2)}) async-start(bf16[64,8,512]{2,1,0:T(8,128)(2,1)} %broadcast_in_dim.17), calls=%async_computation.3 | async-start | bytes 1048576 | tf_op jit(solution)/shard_map/all_to_all | solution.py:303
  57.3 16.7 %all-to-all-done.3 = bf16[64,8,512]{2,1,0:T(8,128)(2,1)S(1)} async-done(((bf16[64,8,512]{2,1,0:T(8,128)(2,1)}), bf16[64,8,512]{2,1,0:T(8,128)(2,1)S(1)}, u32[]{:S(2)}, u32[]{:S(2)}) %all-to-all-start.3) | async-done | bytes 524320 | tf_op jit(solution)/shard_map/all_to_all | solution.py:303
  74.0 1.1 broadcast_in_dim.15
  75.2 5.7 %all-to-all-start = ((bf16[64,2,2048]{2,1,0:T(2,128)(2,1)}), bf16[64,2,2048]{2,1,0:T(2,128)(2,1)S(1)}, u32[]{:S(2)}, u32[]{:S(2)}) async-start(bf16[64,2,2048]{2,1,0:T(2,128)(2,1)} %bitcast.4), calls=%async_computation | async-start | bytes 1048576 | tf_op jit(solution)/shard_map/all_to_all | solution.py:401
  81.3 17.2 %all-to-all-done = bf16[64,2,2048]{2,1,0:T(2,128)(2,1)S(1)} async-done(((bf16[64,2,2048]{2,1,0:T(2,128)(2,1)}), bf16[64,2,2048]{2,1,0:T(2,128)(2,1)S(1)}, u32[]{:S(2)}, u32[]{:S(2)}) %all-to-all-start) | async-done | bytes 524320 | tf_op jit(solution)/shard_map/all_to_all | solution.py:401
  99.3 3.4 %all-to-all-start.5 = ((bf16[4,512,64]{1,2,0:T(8,128)(2,1)}), bf16[4,512,64]{1,2,0:T(8,128)(2,1)S(1)}, u32[]{:S(2)}, u32[]{:S(2)}) async-start(bf16[4,512,64]{1,2,0:T(8,128)(2,1)} %broadcast_in_dim.19), calls=%async_computation.5 | async-start | bytes 524288 | tf_op jit(solution)/shard_map/all_to_all | solution.py:303
  102.9 2.0 %fusion.4 = f32[128,352]{0,1:T(8,128)S(1)} fusion(bf16[128,2048]{1,0:T(8,128)(2,1)S(1)} %reshape.129, bf16[1,2048,352]{1,2,0:T(8,128)(2,1)} %param.34), kind=kOutput, calls=%fused_computation.5 | convolution fusion | flops 184549376 | bytes 2146304 | tf_op jit(solution)/shard_map/dot_general | solution.py:412
  105.5 3.2 %all-to-all-done.5 = bf16[4,512,64]{1,2,0:T(8,128)(2,1)S(1)} async-done(((bf16[4,512,64]{1,2,0:T(8,128)(2,1)}), bf16[4,512,64]{1,2,0:T(8,128)(2,1)S(1)}, u32[]{:S(2)}, u32[]{:S(2)}) %all-to-all-start.5) | async-done | bytes 262176 | tf_op jit(solution)/shard_map/all_to_all | solution.py:303
  108.7 0.8 broadcast_in_dim.16
  109.5 3.5 %all-to-all-start.1 = ((bf16[4,128,352]{1,2,0:T(8,128)(2,1)}), bf16[4,128,352]{1,2,0:T(8,128)(2,1)S(1)}, u32[]{:S(2)}, u32[]{:S(2)}) async-start(bf16[4,128,352]{1,2,0:T(8,128)(2,1)} %broadcast_in_dim.16), calls=%async_computation.1 | async-start | bytes 720896 | tf_op jit(solution)/shard_map/all_to_all | solution.py:303
  113.3 5.7 %all-to-all-done.1 = bf16[4,128,352]{1,2,0:T(8,128)(2,1)S(1)} async-done(((bf16[4,128,352]{1,2,0:T(8,128)(2,1)}), bf16[4,128,352]{1,2,0:T(8,128)(2,1)S(1)}, u32[]{:S(2)}, u32[]{:S(2)}) %all-to-all-start.1) | async-done | bytes 360480 | tf_op jit(solution)/shard_map/all_to_all | solution.py:303
  119.7 3.4 %all-to-all-start.4 = ((bf16[4,512,64]{1,2,0:T(8,128)(2,1)}), bf16[4,512,64]{1,2,0:T(8,128)(2,1)S(1)}, u32[]{:S(2)}, u32[]{:S(2)}) async-start(bf16[4,512,64]{1,2,0:T(8,128)(2,1)} %broadcast_in_dim.18), calls=%async_computation.4 | async-start | bytes 524288 | tf_op jit(solution)/shard_map/all_to_all | solution.py:303
  124.3 4.3 %all-to-all-done.4 = bf16[4,512,64]{1,2,0:T(8,128)(2,1)S(1)} async-done(((bf16[4,512,64]{1,2,0:T(8,128)(2,1)}), bf16[4,512,64]{1,2,0:T(8,128)(2,1)S(1)}, u32[]{:S(2)}, u32[]{:S(2)}) %all-to-all-start.4) | async-done | bytes 262176 | tf_op jit(solution)/shard_map/all_to_all | solution.py:303
  128.6 8.8 %all-to-all-start.2 = ((bf16[64,2,512]{2,1,0:T(2,128)(2,1)}), bf16[64,2,512]{2,1,0:T(2,128)(2,1)S(1)}, u32[]{:S(2)}, u32[]{:S(2)}) async-start(bf16[64,2,512]{2,1,0:T(2,128)(2,1)} %reshape.131), calls=%async_computation.2 | async-start | bytes 262144 | tf_op jit(solution)/shard_map/all_to_all | solution.py:418
  137.4 1.1 fusion.6
  138.6 9.9 %all-to-all-done.2 = bf16[64,2,512]{2,1,0:T(2,128)(2,1)S(1)} async-done(((bf16[64,2,512]{2,1,0:T(2,128)(2,1)}), bf16[64,2,512]{2,1,0:T(2,128)(2,1)S(1)}, u32[]{:S(2)}, u32[]{:S(2)}) %all-to-all-start.2) | async-done | bytes 131104 | tf_op jit(solution)/shard_map/all_to_all | solution.py:418
  148.5 4.5 %all-to-all-start.6 = ((bf16[64,8,512]{2,1,0:T(8,128)(2,1)}), bf16[64,8,512]{2,1,0:T(8,128)(2,1)S(1)}, u32[]{:S(2)}, u32[]{:S(2)}) async-start(bf16[64,8,512]{2,1,0:T(8,128)(2,1)} %fusion.6), calls=%async_computation.6 | async-start | bytes 1048576 | tf_op jit(solution)/shard_map/all_to_all | solution.py:324
  153.6 17.1 %all-to-all-done.6 = bf16[64,8,512]{2,1,0:T(8,128)(2,1)S(1)} async-done(((bf16[64,8,512]{2,1,0:T(8,128)(2,1)}), bf16[64,8,512]{2,1,0:T(8,128)(2,1)S(1)}, u32[]{:S(2)}, u32[]{:S(2)}) %all-to-all-start.6) | async-done | bytes 524320 | tf_op jit(solution)/shard_map/all_to_all | solution.py:324
  171.1 6.5 %all_to_all.41 = f32[4,1,16]{2,1,0:T(1,128)S(1)} all-to-all(f32[4,1,16]{2,1,0:T(1,128)S(1)} %broadcast_in_dim.20), channel_id=1, replica_groups=mesh['ep'=64,'tp'=4] {'tp'}, dimensions={0} | all-to-all | bytes 512 | tf_op jit(solution)/shard_map/all_to_all | solution.py:303
  (73 shorter events, 12.4 us)
Async XLA Ops:
  0.0 123.1 %copy-start = (bf16[1,1408,512]{2,1,0:T(8,128)(2,1)S(1)}, bf16[1,1408,512]{2,1,0:T(8,128)(2,1)}, u32[]{:S(2)}) copy-start(bf16[1,1408,512]{2,1,0:T(8,128)(2,1)} %param.36) | copy-start | bytes 4325380
  1.0 1.6 copy-start.1
  2.6 1.6 copy-start.2
  4.2 0.8 copy-start.3
  4.9 0.8 copy-start.4
  5.7 0.7 copy-start.5
  6.4 0.7 copy-start.6
  7.1 0.7 copy-start.7
  7.8 0.7 copy-start.8
  49.7 6.7 %copy-start.15 = (s32[8,2]{0,1:T(2,128)S(1)}, s32[8,2]{0,1:T(2,128)}, u32[]{:S(2)}) copy-start(s32[8,2]{0,1:T(2,128)} %param.32) | copy-start | bytes 196
  50.6 23.5 %all-to-all-start.3 = ((bf16[64,8,512]{2,1,0:T(8,128)(2,1)}), bf16[64,8,512]{2,1,0:T(8,128)(2,1)S(1)}, u32[]{:S(2)}, u32[]{:S(2)}) async-start(bf16[64,8,512]{2,1,0:T(8,128)(2,1)} %broadcast_in_dim.17), calls=%async_computation.3 | async-start | bytes 1048576 | tf_op jit(solution)/shard_map/all_to_all | solution.py:303
  56.4 24.7 %copy-start.11 = (bf16[512,64]{0,1:T(8,128)(2,1)S(1)}, bf16[512,64]{0,1:T(8,128)(2,1)}, u32[]{:S(2)}) copy-start(bf16[512,64]{0,1:T(8,128)(2,1)} %param.38) | copy-start | bytes 196612
  75.2 23.4 %all-to-all-start = ((bf16[64,2,2048]{2,1,0:T(2,128)(2,1)}), bf16[64,2,2048]{2,1,0:T(2,128)(2,1)S(1)}, u32[]{:S(2)}, u32[]{:S(2)}) async-start(bf16[64,2,2048]{2,1,0:T(2,128)(2,1)} %bitcast.4), calls=%async_computation | async-start | bytes 1048576 | tf_op jit(solution)/shard_map/all_to_all | solution.py:401
  99.3 9.5 %all-to-all-start.5 = ((bf16[4,512,64]{1,2,0:T(8,128)(2,1)}), bf16[4,512,64]{1,2,0:T(8,128)(2,1)S(1)}, u32[]{:S(2)}, u32[]{:S(2)}) async-start(bf16[4,512,64]{1,2,0:T(8,128)(2,1)} %broadcast_in_dim.19), calls=%async_computation.5 | async-start | bytes 524288 | tf_op jit(solution)/shard_map/all_to_all | solution.py:303
  102.9 2.0 %copy-start.17 = (bf16[1,2048,352]{1,2,0:T(8,128)(2,1)S(1)}, bf16[1,2048,352]{1,2,0:T(8,128)(2,1)}, u32[]{:S(2)}) copy-start(bf16[1,2048,352]{1,2,0:T(8,128)(2,1)} %param.35) | copy-start | bytes 4325380
  104.9 8.0 %copy-start.12 = (bf16[512,64]{0,1:T(8,128)(2,1)S(1)}, bf16[512,64]{0,1:T(8,128)(2,1)}, u32[]{:S(2)}) copy-start(bf16[512,64]{0,1:T(8,128)(2,1)} %param.37) | copy-start | bytes 196612
  109.5 9.5 %all-to-all-start.1 = ((bf16[4,128,352]{1,2,0:T(8,128)(2,1)}), bf16[4,128,352]{1,2,0:T(8,128)(2,1)S(1)}, u32[]{:S(2)}, u32[]{:S(2)}) async-start(bf16[4,128,352]{1,2,0:T(8,128)(2,1)} %broadcast_in_dim.16), calls=%async_computation.1 | async-start | bytes 720896 | tf_op jit(solution)/shard_map/all_to_all | solution.py:303
  119.7 8.9 %all-to-all-start.4 = ((bf16[4,512,64]{1,2,0:T(8,128)(2,1)}), bf16[4,512,64]{1,2,0:T(8,128)(2,1)S(1)}, u32[]{:S(2)}, u32[]{:S(2)}) async-start(bf16[4,512,64]{1,2,0:T(8,128)(2,1)} %broadcast_in_dim.18), calls=%async_computation.4 | async-start | bytes 524288 | tf_op jit(solution)/shard_map/all_to_all | solution.py:303
  123.1 14.3 %copy-start.13 = (bf16[64,512]{1,0:T(8,128)(2,1)S(1)}, bf16[64,512]{1,0:T(8,128)(2,1)}, u32[]{:S(2)}) copy-start(bf16[64,512]{1,0:T(8,128)(2,1)} %param.39) | copy-start | bytes 196612
  123.5 29.4 %copy-start.14 = (f32[2048]{0:T(1024)S(1)}, f32[2048]{0:T(1024)}, u32[]{:S(2)}) copy-start(f32[2048]{0:T(1024)} %param.40) | copy-start | bytes 24580
  124.2 29.0 %copy-start.18 = (f32[8,2]{0,1:T(2,128)S(1)}, f32[8,2]{0,1:T(2,128)}, u32[]{:S(2)}) copy-start(f32[8,2]{0,1:T(2,128)} %param.33) | copy-start | bytes 196
  128.6 19.9 %all-to-all-start.2 = ((bf16[64,2,512]{2,1,0:T(2,128)(2,1)}), bf16[64,2,512]{2,1,0:T(2,128)(2,1)S(1)}, u32[]{:S(2)}, u32[]{:S(2)}) async-start(bf16[64,2,512]{2,1,0:T(2,128)(2,1)} %reshape.131), calls=%async_computation.2 | async-start | bytes 262144 | tf_op jit(solution)/shard_map/all_to_all | solution.py:418
  137.4 40.3 %copy-start.16 = (f32[512]{0:T(512)S(1)}, f32[512]{0:T(512)}, u32[]{:S(2)}) copy-start(f32[512]{0:T(512)} %param.41) | copy-start | bytes 6148
  148.5 22.3 %all-to-all-start.6 = ((bf16[64,8,512]{2,1,0:T(8,128)(2,1)}), bf16[64,8,512]{2,1,0:T(8,128)(2,1)S(1)}, u32[]{:S(2)}, u32[]{:S(2)}) async-start(bf16[64,8,512]{2,1,0:T(8,128)(2,1)} %fusion.6), calls=%async_computation.6 | async-start | bytes 1048576 | tf_op jit(solution)/shard_map/all_to_all | solution.py:324
  (2 other events, 1.3 us)

commit v2 on v1

v2 whole, which is shorter than its diff:
```python
from types import SimpleNamespace

import jax
import jax.numpy as jnp
import numpy as np
from jax import lax
from jax.experimental import pallas as pl
from jax.experimental.pallas import tpu as pltpu
from jax.sharding import PartitionSpec as P

EPS = 1e-05

NZ, NQ, NT = 8, 8, 4
MESH_ID = pl.DeviceIdType.MESH
F32 = jnp.float32
ONE = np.ones((2, 8), np.float32)
BF16 = jnp.bfloat16
NT_DIMS = (((1,), (1,)), ((), ()))


def dot(a, b):
    return jnp.dot(a, b, preferred_element_type=F32)


def dot_nt(a, b):
    return lax.dot_general(a, b, NT_DIMS, preferred_element_type=F32)


def stacked(ref, n):
    return jnp.concatenate([ref[i].astype(F32) for i in range(n)], axis=0).astype(BF16)


SCRATCH = dict(
    tok_v=pltpu.VMEM((8, 2048), BF16),
    tokg=pltpu.VMEM((NZ, 8, 256), BF16),
    wg=pltpu.VMEM((256, 768), BF16),
    wog=pltpu.VMEM((256, 512), BF16),
    kbuf=pltpu.VMEM((8, 1024, 128), BF16),
    vbuf=pltpu.VMEM((8, 1024, 128), BF16),
    fg_v=pltpu.VMEM((1, 2048), F32),
    hg_v=pltpu.VMEM((1, 128), F32),
    sw_v=pltpu.VMEM((1, 2048), F32),
    fin_v=pltpu.VMEM((1, 512), F32),
    pbuf=pltpu.VMEM((NZ, 8, 768), F32),
    precv=pltpu.VMEM((NZ, 8, 768), F32),
    qv=pltpu.VMEM((8, 768), F32),
    qs=pltpu.VMEM((8, 8, 128), F32),
    nv=pltpu.VMEM((8, 512), F32),
    ng=pltpu.VMEM((NQ, 8, 512), BF16),
    gbuf=pltpu.VMEM((NQ, 8, 256), BF16),
    attr=pltpu.VMEM((NT, NQ, 8, 256), BF16),
    eg=pltpu.VMEM((352, 2048), BF16),
    eu=pltpu.VMEM((352, 2048), BF16),
    ed=pltpu.VMEM((1408, 512), BF16),
    dw=pltpu.VMEM((3, 512, 512), BF16),
    hid=pltpu.VMEM((8, 2048), F32),
    sel=pltpu.VMEM((256, 256), BF16),
    selt=pltpu.VMEM((256, 256), BF16),
    pk=pltpu.VMEM((16, 8, 512), BF16),
    rows=pltpu.VMEM((2, 32, 8, 512), BF16),
    hg=pltpu.VMEM((2, NT, 64, 352), BF16),
    rb=pltpu.VMEM((2, 32, 8, 128), BF16),
    ret=pltpu.VMEM((64, 8, 128), BF16),
    dg=pltpu.VMEM((NZ, 8, 512), BF16),
    gp=pltpu.VMEM((NT, 16, 1024), BF16),
    gr=pltpu.VMEM((NT, 16, 1024), BF16),
    dh=pltpu.VMEM((NT, 16, 512), BF16),
    op=pltpu.VMEM((NZ, 8, 512), BF16),
    orv=pltpu.VMEM((NZ, 8, 512), BF16),
    st=pltpu.VMEM((NT, 8, 128), F32),
    lsem=pltpu.SemaphoreType.DMA((18,)),
    s_wg=pltpu.SemaphoreType.DMA((NQ,)),
    r_wg=pltpu.SemaphoreType.DMA((NQ,)),
    s_tok=pltpu.SemaphoreType.DMA((NZ,)),
    r_tok=pltpu.SemaphoreType.DMA((NZ,)),
    s_wo=pltpu.SemaphoreType.DMA((NZ,)),
    r_wo=pltpu.SemaphoreType.DMA((NZ,)),
    s_p=pltpu.SemaphoreType.DMA((NZ,)),
    r_p=pltpu.SemaphoreType.DMA((NZ,)),
    s_n=pltpu.SemaphoreType.DMA((NQ,)),
    r_n=pltpu.SemaphoreType.DMA((NQ,)),
    s_a=pltpu.SemaphoreType.DMA((NT * NQ,)),
    r_a=pltpu.SemaphoreType.DMA((NT * NQ,)),
    s_dw=pltpu.SemaphoreType.DMA((9,)),
    r_dw=pltpu.SemaphoreType.DMA((9,)),
    s_df=pltpu.SemaphoreType.DMA((3,)),
    r_df=pltpu.SemaphoreType.DMA((3,)),
    s_dp=pltpu.SemaphoreType.DMA((32,)),
    r_dp=pltpu.SemaphoreType.DMA((32,)),
    s_sw=pltpu.SemaphoreType.DMA((1,)),
    r_sw=pltpu.SemaphoreType.DMA((1,)),
    s_dg=pltpu.SemaphoreType.DMA((NZ,)),
    r_dg=pltpu.SemaphoreType.DMA((NZ,)),
    s_gr=pltpu.SemaphoreType.DMA((NT,)),
    r_gr=pltpu.SemaphoreType.DMA((NT,)),
    s_dh=pltpu.SemaphoreType.DMA((NT,)),
    r_dh=pltpu.SemaphoreType.DMA((NT,)),
    s_or=pltpu.SemaphoreType.DMA((NZ,)),
    r_or=pltpu.SemaphoreType.DMA((NZ,)),
    s_hg=pltpu.SemaphoreType.DMA((2 * NT,)),
    r_hg=pltpu.SemaphoreType.DMA((2 * NT,)),
    s_rt=pltpu.SemaphoreType.DMA((64,)),
    r_rt=pltpu.SemaphoreType.DMA((64,)),
    s_st=pltpu.SemaphoreType.DMA((NT,)),
    r_st=pltpu.SemaphoreType.DMA((NT,)),
)


def remote(src, dst, send, recv, ep, tp):
    return pltpu.make_async_remote_copy(
        src_ref=src, dst_ref=dst, send_sem=send, recv_sem=recv,
        device_id=(ep, tp), device_id_type=MESH_ID,
    )


def where_am_i():
    ep, tp = lax.axis_index("ep"), lax.axis_index("tp")
    return ep // NQ, lax.rem(ep, NQ), tp


def placing(e, slot, b, routing, weights):
    rank = jnp.zeros(e.shape, jnp.int32)
    share = jnp.zeros(e.shape, F32)
    for i in range(8):
        first, second = e == routing[0, i], e == routing[1, i]
        rank = rank + jnp.where((first | second) & (b > i), 1, 0)
        mine = jnp.where(first, weights[0, i], jnp.where(second, weights[1, i], 0.0))
        share = jnp.where(b == i, mine, share)
    return jnp.where(rank == slot, share, 0.0)


def silu(v):
    return v / (1.0 + jnp.exp(-v))


def iota2(shape):
    return tuple(lax.broadcasted_iota(jnp.int32, shape, i) for i in range(2))


def layer_kernel(
    lengths, mixw, routing, rweights, tokens, keys, values, wq, wk, wv, wout, hgain, fgain,
    egate, eup, edown, dgate, dup, ddown, switchv, final, out, *scratch
):
    s = SimpleNamespace(**dict(zip(SCRATCH, scratch)))
    z, q, y = where_am_i()
    x, core = q // 2, lax.rem(q, 2)
    me = z * NQ + q
    chip = me // 2
    sent = []

    def go(c):
        c.start()
        sent.append(c)
        return c

    qrow = pl.multiple_of(q * 32, 32)
    zrow = pl.multiple_of(z * 32, 32)
    first = [
        pltpu.make_async_copy(tokens, s.tok_v, s.lsem.at[0]),
        pltpu.make_async_copy(wq, s.wg.at[pl.ds(qrow, 32), pl.ds(0, 512)], s.lsem.at[1]),
        pltpu.make_async_copy(wk, s.wg.at[pl.ds(qrow, 32), pl.ds(512, 128)], s.lsem.at[2]),
        pltpu.make_async_copy(wv, s.wg.at[pl.ds(qrow, 32), pl.ds(640, 128)], s.lsem.at[3]),
        pltpu.make_async_copy(wout, s.wog.at[pl.ds(zrow, 32), :], s.lsem.at[4]),
    ]
    later = [
        pltpu.make_async_copy(keys, s.kbuf, s.lsem.at[5]),
        pltpu.make_async_copy(values, s.vbuf, s.lsem.at[6]),
        pltpu.make_async_copy(fgain, s.fg_v, s.lsem.at[7]),
        pltpu.make_async_copy(hgain, s.hg_v, s.lsem.at[8]),
    ]
    drow = pl.multiple_of((core * 4 + x) * 64, 64)
    dense = [
        pltpu.make_async_copy(w, s.dw.at[i, pl.ds(drow, 64), :], s.lsem.at[9 + i])
        for i, w in enumerate((dgate, dup, ddown))
    ]
    last = [
        pltpu.make_async_copy(egate, s.eg, s.lsem.at[12]),
        pltpu.make_async_copy(eup, s.eu, s.lsem.at[13]),
        pltpu.make_async_copy(edown, s.ed, s.lsem.at[14]),
        pltpu.make_async_copy(switchv, s.sw_v, s.lsem.at[15]),
        pltpu.make_async_copy(final, s.fin_v, s.lsem.at[16]),
    ]
    for c in first:
        c.start()

    barrier = pltpu.get_barrier_semaphore()
    for d in range(1, NZ):
        pl.semaphore_signal(
            barrier, inc=1, device_id=(lax.rem(z + d, NZ) * NQ + q, y), device_id_type=MESH_ID
        )
    for d in range(1, NQ):
        pl.semaphore_signal(
            barrier, inc=1, device_id=(z * NQ + lax.rem(q + d, NQ), y), device_id_type=MESH_ID
        )
    for d in range(1, NT):
        pl.semaphore_signal(
            barrier, inc=1, device_id=(me, lax.rem(y + d, NT)), device_id_type=MESH_ID
        )
    for c in dense + later + last:
        c.start()
    i, j = iota2((256, 256))
    s.sel[...] = jnp.where(j == (i % 32) * 8 + (i // 64) * 2 + (i // 32) % 2, 1.0, 0.0).astype(BF16)
    s.selt[...] = jnp.where(i == (j % 32) * 8 + (j // 64) * 2 + (j // 32) % 2, 1.0, 0.0).astype(BF16)
    for c in first + dense:
        c.wait()
    pl.semaphore_wait(barrier, NZ - 1 + NQ - 1 + NT - 1)

    wg_copies, tok_copies, wo_copies = [], [], []
    for d in range(1, NZ):
        zz = lax.rem(z + d, NZ)
        c = remote(
            s.tok_v.at[:, pl.ds(pl.multiple_of(zz * 256, 256), 256)], s.tokg.at[z],
            s.s_tok.at[d], s.r_tok.at[d], zz * NQ + q, y,
        )
        c.start()
        tok_copies.append(c)
    for d in range(1, NQ):
        mine = s.wg.at[pl.ds(qrow, 32), :]
        c = remote(mine, mine, s.s_wg.at[d], s.r_wg.at[d], z * NQ + lax.rem(q + d, NQ), y)
        c.start()
        wg_copies.append(c)
    for d in range(1, NZ):
        mine = s.wog.at[pl.ds(zrow, 32), :]
        c = remote(mine, mine, s.s_wo.at[d], s.r_wo.at[d], lax.rem(z + d, NZ) * NQ + q, y)
        c.start()
        wo_copies.append(c)
    dw_copies = []
    for i in range(3):
        for d in range(1, 4):
            mine = s.dw.at[i, pl.ds(drow, 64), :]
            k = i * 3 + d - 1
            dw_copies.append(go(remote(
                mine, mine, s.s_dw.at[k], s.r_dw.at[k], z * NQ + lax.rem(q + 2 * d, NQ), y
            )))
    s.tokg[z] = s.tok_v[:, pl.ds(pl.multiple_of(z * 256, 256), 256)]

    for c in tok_copies + wg_copies:
        c.wait_recv()
    part = dot(stacked(s.tokg, NZ), s.wg[...])
    for i in range(NZ):
        s.pbuf[i] = part[i * 8:(i + 1) * 8]
    p_copies = []
    for d in range(1, NZ):
        zz = lax.rem(z + d, NZ)
        c = remote(s.pbuf.at[zz], s.precv.at[z], s.s_p.at[d], s.r_p.at[d], zz * NQ + q, y)
        c.start()
        p_copies.append(c)
    s.precv[z] = s.pbuf[z]
    for c in p_copies:
        c.wait_recv()
    total = s.precv[0]
    for i in range(1, NZ):
        total = total + s.precv[i]
    s.qv[...] = total.astype(BF16).astype(F32)
    for b in range(8):
        for r in range(4):
            row = s.qv[b:b + 1, r * 128:(r + 1) * 128]
            s.qs[b, r:r + 1, :] = row
            s.qs[b, r + 4:r + 5, :] = row

    for c in later:
        c.wait()
    sub = lax.broadcasted_iota(jnp.int32, (8, 128), 0)
    lane = lax.broadcasted_iota(jnp.int32, (8, 128), 1)
    half = (sub >= 4) == (lane >= 64)
    col = lax.broadcasted_iota(jnp.int32, (8, 1024), 1)
    rows1 = lax.broadcasted_iota(jnp.int32, (8, 1), 0)
    lam = jnp.zeros((8, 1), F32)
    for r in range(4):
        lam = jnp.where(rows1 == r + 4, mixw[r], lam)
    weight = jnp.where(rows1 < 4, 1.0, -lam)
    for b in range(8):
        q8 = jnp.where(half, s.qs[b], 0.0)
        knew = s.qv[b:b + 1, 512:640]
        vnew = s.qv[b:b + 1, 640:768]
        sc = dot_nt(q8.astype(BF16), s.kbuf[b]) * 0.125
        own = jnp.sum(q8 * knew, axis=1, keepdims=True) * 0.125
        sc = jnp.where(col < lengths[b], sc, -jnp.inf)
        top = jnp.maximum(jnp.max(sc, axis=1, keepdims=True), own)
        e = jnp.exp(sc - top)
        eo = jnp.exp(own - top)
        scale = weight / (jnp.sum(e, axis=1, keepdims=True) + eo)
        t = e * scale
        mix = (t + pltpu.roll(t, 4, 0)).astype(BF16)
        to = jnp.broadcast_to(eo * scale, (8, 128))
        mix_own = (to + pltpu.roll(to, 4, 0)).astype(BF16).astype(F32)
        ho = dot(mix, s.vbuf[b]) + mix_own * vnew
        square = jnp.mean(ho * ho, axis=1, keepdims=True)
        n8 = ho * lax.rsqrt(square + EPS) * s.hg_v[...]
        for r in range(4):
            s.nv[b:b + 1, r * 128:(r + 1) * 128] = n8[r:r + 1, :]
    s.ng[q] = s.nv[...].astype(BF16)
    n_copies = []
    for d in range(1, NQ):
        c = remote(
            s.ng.at[q], s.ng.at[q], s.s_n.at[d], s.r_n.at[d], z * NQ + lax.rem(q + d, NQ), y
        )
        c.start()
        n_copies.append(c)
    for c in wo_copies + n_copies:
        c.wait_recv()
    group = dot_nt(stacked(s.ng, NQ), s.wog[...])
    for i in range(NQ):
        s.gbuf[i] = group[i * 8:(i + 1) * 8].astype(BF16)
    a_copies = []
    for dy in range(NT):
        for dq in range(NQ):
            if dy or dq:
                qq = lax.rem(q + dq, NQ)
                c = remote(
                    s.gbuf.at[qq], s.attr.at[y, q], s.s_a.at[dy * NQ + dq],
                    s.r_a.at[dy * NQ + dq], z * NQ + qq, lax.rem(y + dy, NT),
                )
                c.start()
                a_copies.append(c)
    s.attr[y, q] = s.gbuf[q]
    for c in dw_copies:
        c.wait_recv()
    df_copies = []
    other = me + 1 - 2 * core
    for i in range(3):
        mine = s.dw.at[i, pl.ds(pl.multiple_of(core * 256, 256), 256), :]
        df_copies.append(go(remote(mine, mine, s.s_df.at[i], s.r_df.at[i], other, y)))
    for c in a_copies:
        c.wait_recv()
    parts = []
    for i in range(NQ):
        acc = s.attr[0, i].astype(F32)
        for t in range(1, NT):
            acc = acc + s.attr[t, i].astype(F32)
        parts.append(acc)
    lane32 = lane // 32
    tiles = []
    for zz in range(NZ):
        for h in range(2):
            tile = None
            for k in range(4):
                off = zz * 32
                piece = parts[h * 4 + k][:, (off // 128) * 128:(off // 128) * 128 + 128]
                shift = (k * 32 - off % 128) % 128
                if shift:
                    piece = pltpu.roll(piece, shift, 1)
                tile = piece if tile is None else jnp.where(lane32 == k, piece, tile)
            tiles.append(tile)
    x = s.tok_v[...].astype(F32) + jnp.concatenate(tiles, axis=1)
    mean = jnp.mean(x, axis=1, keepdims=True)
    xc = x - mean
    spread = jnp.mean(xc * xc, axis=1, keepdims=True)
    hidden = (xc * lax.rsqrt(spread + EPS) * s.fg_v[...]).astype(BF16)
    hid32 = hidden.astype(F32)
    s.hid[...] = hid32

    i, j = iota2((128, 32))
    ones = placing(i // 8, i % 2, j % 8, routing, ONE)
    place = jnp.where((i // 2) % 4 == j // 8, ones, 0.0).astype(BF16)
    quarters = jnp.concatenate([hid32[:, t * 512:(t + 1) * 512] for t in range(4)], axis=0)
    packed = dot(place, quarters.astype(BF16))
    for e in range(16):
        s.pk[e] = packed[e * 8:(e + 1) * 8].astype(BF16)
    dp_copies = []
    for d in range(1, 32):
        to = lax.rem(chip + d, 32)
        dp_copies.append(go(remote(
            s.pk.at[to // 2], s.rows.at[0, chip], s.s_dp.at[d], s.r_dp.at[d], to * 2 + core, y
        )))
    s.rows[0, chip] = s.pk[chip // 2]

    s.dg[z] = s.hid[:, pl.ds(pl.multiple_of(y * 512, 512), 512)].astype(BF16)
    dg_copies = [
        go(remote(
            s.dg.at[z], s.dg.at[z], s.s_dg.at[d], s.r_dg.at[d], lax.rem(z + d, NZ) * NQ + q, y
        ))
        for d in range(1, NZ)
    ]
    for c in last:
        c.wait()
    i, j = iota2((32, 128))
    shares = placing(j // 8, j % 2, i % 8, routing, rweights)
    shares = jnp.where((j // 2) % 4 == i // 8, shares, 0.0)
    switch = 1.0 / (1.0 + jnp.exp(-jnp.sum(hid32 * s.sw_v[...], axis=1, keepdims=True)))

    for c in df_copies + dg_copies:
        c.wait_recv()
    group = stacked(s.dg, NZ)
    for k in range(2):
        part = dot_nt(group, s.dw[k]).astype(BF16)
        for t in range(NT):
            s.gp[t, :, k * 512:(k + 1) * 512] = part[t * 16:(t + 1) * 16]
    gr_copies = []
    for d in range(1, NT):
        to = lax.rem(y + d, NT)
        gr_copies.append(go(remote(
            s.gp.at[to], s.gr.at[y], s.s_gr.at[d], s.r_gr.at[d], me, to
        )))
    s.gr[y] = s.gp[y]

    def expert_half(h):
        block = dot(s.sel[...], jnp.concatenate(
            [s.rows[h, i].astype(F32) for i in range(32)], axis=0).astype(BF16)).astype(BF16)
        wide = jnp.concatenate([block[t * 64:(t + 1) * 64] for t in range(4)], axis=1)
        gate, up = dot_nt(wide, s.eg[...]), dot_nt(wide, s.eu[...])
        s.hg[h, y] = (silu(gate) * up).astype(BF16)
        return [
            go(remote(
                s.hg.at[h, y], s.hg.at[h, y], s.s_hg.at[h * NT + d], s.r_hg.at[h * NT + d],
                me, lax.rem(y + d, NT),
            ))
            for d in range(1, NT)
        ]

    for c in dp_copies:
        c.wait_recv()
    swap = go(remote(s.rows.at[0], s.rows.at[1], s.s_sw.at[0], s.r_sw.at[0], other, y))
    hg_copies = [expert_half(0)]

    for c in gr_copies:
        c.wait_recv()
    pre = s.gr[0].astype(F32)
    for t in range(1, NT):
        pre = pre + s.gr[t].astype(F32)
    s.dh[y] = (silu(pre[:, :512]) * pre[:, 512:]).astype(BF16)
    dh_copies = [
        go(remote(
            s.dh.at[y], s.dh.at[y], s.s_dh.at[d], s.r_dh.at[d], me, lax.rem(y + d, NT)
        ))
        for d in range(1, NT)
    ]

    swap.wait_recv()
    hg_copies.append(expert_half(1))

    for c in dh_copies:
        c.wait_recv()
    part = dot(jnp.concatenate([s.dh[t] for t in range(NT)], axis=0), s.dw[2])
    for i in range(NZ):
        s.op[i] = part[i * 8:(i + 1) * 8].astype(BF16)
    or_copies = []
    for d in range(1, NZ):
        to = lax.rem(z + d, NZ)
        or_copies.append(go(remote(
            s.op.at[to], s.orv.at[z], s.s_or.at[d], s.r_or.at[d], to * NQ + q, y
        )))
    s.orv[z] = s.op[z]

    rt_copies = []
    for h in range(2):
        for c in hg_copies[h]:
            c.wait_recv()
        acc = dot(s.hg[h, 0], s.ed[0:352])
        for t in range(1, NT):
            acc = acc + dot(s.hg[h, t], s.ed[t * 352:(t + 1) * 352])
        acc = acc.astype(BF16)
        tall = jnp.concatenate([acc[:, t * 128:(t + 1) * 128] for t in range(4)], axis=0)
        back = dot(s.selt[...], tall)
        for i in range(32):
            s.rb[h, i] = back[i * 8:(i + 1) * 8].astype(BF16)
        there = core if h == 0 else 1 - core
        for d in range(32):
            to = lax.rem(chip + d, 32)
            if h or d:
                k = h * 32 + d
                rt_copies.append(go(remote(
                    s.rb.at[h, to], s.ret.at[me], s.s_rt.at[k], s.r_rt.at[k], to * 2 + there, y
                )))
            else:
                s.ret[me] = s.rb[0, chip]

    for c in or_copies:
        c.wait_recv()
    dense_out = s.orv[0].astype(F32)
    for i in range(1, NZ):
        dense_out = dense_out + s.orv[i].astype(F32)
    dense_out = dense_out.astype(BF16).astype(F32)
    combined = s.hid[:, pl.ds(pl.multiple_of(y * 512, 512), 512)] + switch * dense_out

    for c in rt_copies:
        c.wait_recv()
    sums = []
    for e in range(16):
        acc = s.ret[4 * e].astype(F32)
        for t in range(1, 4):
            acc = acc + s.ret[4 * e + t].astype(F32)
        sums.append(acc)
    routed = jnp.dot(
        shares, jnp.concatenate(sums, axis=0), preferred_element_type=F32,
        precision=lax.Precision.HIGHEST,
    )
    combined = combined + jnp.concatenate([routed[t * 8:(t + 1) * 8] for t in range(4)], axis=1)
    total = jnp.sum(combined, axis=1, keepdims=True)
    square = jnp.sum(combined * combined, axis=1, keepdims=True)
    s.st[y] = jnp.where(lane < 64, total, square)
    st_copies = [
        go(remote(
            s.st.at[y], s.st.at[y], s.s_st.at[d], s.r_st.at[d], me, lax.rem(y + d, NT)
        ))
        for d in range(1, NT)
    ]
    for c in st_copies:
        c.wait_recv()
    stats = s.st[0] + s.st[1] + s.st[2] + s.st[3]
    mean = stats[:, 0:1] / 2048
    spread = stats[:, 64:65] / 2048 - mean * mean
    result = (combined - mean) * lax.rsqrt(spread + EPS) * s.fin_v[...]
    out[...] = result.astype(BF16)
    for c in tok_copies + wg_copies + wo_copies + p_copies + n_copies + a_copies + sent:
        c.wait_send()


def body(
    tokens, lengths, cache_keys, cache_values, w_query, w_key, w_value, mix_weight, head_gain,
    w_out, first_gain, routing, route_weights, expert_gate, expert_up, expert_down, dense_gate,
    dense_up, dense_down, switch_vector, final_gain,
):
    hbm = pl.BlockSpec(memory_space=pltpu.HBM)
    smem = pl.BlockSpec(memory_space=pltpu.SMEM)
    return pl.pallas_call(
        layer_kernel,
        out_shape=jax.ShapeDtypeStruct((8, 512), BF16),
        in_specs=[smem] * 4 + [hbm] * 17,
        out_specs=pl.BlockSpec(memory_space=pltpu.VMEM),
        scratch_shapes=list(SCRATCH.values()),
        compiler_params=pltpu.CompilerParams(
            collective_id=0, has_side_effects=True, vmem_limit_bytes=60 * 1024 * 1024
        ),
        name="layer",
    )(
        lengths, mix_weight, routing.T, route_weights.T, tokens,
        cache_keys.reshape(8, 1024, 128), cache_values.reshape(8, 1024, 128),
        w_query, w_key, w_value, w_out.T, head_gain.reshape(1, 128),
        first_gain.reshape(1, 2048), expert_gate[0].T, expert_up[0].T, expert_down[0],
        dense_gate.T, dense_up.T, dense_down, switch_vector.reshape(1, 2048),
        final_gain.reshape(1, 512),
    )


def solution(mesh):
    placed = (
        P("ep", None),
        P("ep"),
        P("ep", "tp", None, None),
        P("ep", "tp", None, None),
        P("ep", "tp"),
        P("ep", "tp"),
        P("ep", "tp"),
        P("tp"),
        P(),
        P("tp", "ep"),
        P(),
        P("ep", None),
        P("ep", None),
        P("ep", None, "tp"),
        P("ep", None, "tp"),
        P("ep", None, "tp"),
        P("tp", "ep"),
        P("tp", "ep"),
        P("ep", "tp"),
        P(),
        P("tp"),
    )
    return jax.shard_map(body, mesh=mesh, in_specs=placed, out_specs=P("ep", "tp"), check_vma=False)
```

time: 179 us -> 74.9 us (0.42)
  waiting for transfers between devices: 74.3 us -> 0 us
  starting transfers between devices: 35 us -> 0 us
  Pallas kernels: 39.9 us -> 73.5 us
  local copies, waits for them, and re-layouts: 15.4 us -> 1.3 us
  blocking collectives: 6.46 us -> 0 us
  matrix products: 5.1 us -> 0 us
  other arithmetic: 1.85 us -> 0 us
    all_to_all x7 -> x0, waiting for transfers between devices: 74.3 us -> none  [the longest x4 30 us: from_everyone(): lax.all_to_all(jnp.broadcast_to(shard[None], (devices, *shard.shape)), ax...]
    all_to_all x7 -> x0, starting transfers between devices: 35 us -> none  [the longest x4 16.1 us: from_everyone(): lax.all_to_all(jnp.broadcast_to(shard[None], (devices, *shard.shape)), ax...]
    pallas_call x1, Pallas kernels: 39.9 us -> 73.5 us  [body(): pl.pallas_call(layer_kernel, out_shape=jax.ShapeDtypeStruct((8, 512), BF1...]
    unnamed x40 -> x1, local copies, waits for them, and re-layouts: 9.87 us -> 1.3 us
    all_to_all x1 -> x0, blocking collectives: 6.46 us -> none  [from_everyone(): lax.all_to_all(jnp.broadcast_to(shard[None], (devices, *shard.shape)), ax...]
    dot_general x8 -> x0, matrix products: 5.1 us -> none  [the longest x1 2.01 us: body(): gate = jnp.dot(rows, expert_gate[0], preferred_element_type=f32)]
    broadcast_in_dim x7 -> x0, local copies, waits for them, and re-layouts: 4.17 us -> none  [the longest x5 3.02 us: from_everyone(): jnp.broadcast_to(shard[None], (devices, *shard.shape))]
  transfers between devices with their start and end apart: 7 -> 0, of which waited for: 7 -> 0; matrix products, arithmetic and copies ran while one was open for 4% -> 0% of each run, Pallas kernels for 0% -> 0%
where the time goes in v2:
time: 74.9 us; the launch traced here: 74.8 us
  Pallas kernels  73.5 us (98%)
  local copies, waits for them, and re-layouts  1.3 us (2%)
    pallas_call x1, Pallas kernels, body(): pl.pallas_call(layer_kernel, out_shape=jax.ShapeDtypeStruct((8, 512), BF1...  73.5 us

profile of v2, /device:TPU:1, one launch (start us, length us, event | category | flops | bytes accessed | tf_op | source)
XLA Modules:
  0.0 74.8 jit_solution(14615986340726852434)
XLA Ops:
  0.0 73.5 %layer.1 = bf16[8,512]{1,0:T(8,128)(2,1)} custom-call(s32[8]{0:T(128)} %lengths.1, f32[4]{0:T(128)} %mixw.1, s32[2,8]{1,0:T(2,128)} %bitcast.29, f32[2,8]{1,0:T(2,128)} %bitcast.30, bf16[8,2048]{1,0:T(8,128)(2,1)} %tokens.1, bf16[8,1024,128]{2,1,0:T(8,128)(2,1)} %bitcast.18, bf16[8,1024,128]{2,1,0:T(8,128)(2,1)} %bitcast.19, bf16[32,512]{1,0:T(8,128)(2,1)} %wq.1, ...), custom_call_target="tpu_custom_call" | custom-call | tf_op jit(solution)/shard_map/layer/pallas_call | solution.py:516
  73.5 1.3 %copy.23 = bf16[8,512]{1,0:T(8,128)(2,1)} copy(bf16[8,512]{1,0:T(8,128)(2,1)} %layer.1) | data formatting | bytes 16384

commit v3 on v2

--- a/solution.py
+++ b/solution.py
@@ -11,6 +11,10 @@
 EPS = 1e-05
 
 NZ, NQ, NT = 8, 8, 4
+FAR_Z = (4, 3, 5, 2, 6, 1, 7)
+FAR_Q = (4, 5, 3, 2, 6, 7, 1)
+FAR_X = (2, 1, 3)
+FAR_T = (2, 1, 3)
 MESH_ID = pl.DeviceIdType.MESH
 F32 = jnp.float32
 ONE = np.ones((2, 8), np.float32)
@@ -32,8 +36,9 @@
 
 SCRATCH = dict(
     tok_v=pltpu.VMEM((8, 2048), BF16),
-    tokg=pltpu.VMEM((NZ, 8, 256), BF16),
-    wg=pltpu.VMEM((256, 768), BF16),
+    tokg=pltpu.VMEM((2 * NZ, 8, 256), BF16),
+    wmine=pltpu.VMEM((32, 768), BF16),
+    wg=pltpu.VMEM((256, 384), BF16),
     wog=pltpu.VMEM((256, 512), BF16),
     kbuf=pltpu.VMEM((8, 1024, 128), BF16),
     vbuf=pltpu.VMEM((8, 1024, 128), BF16),
@@ -41,8 +46,8 @@
     hg_v=pltpu.VMEM((1, 128), F32),
     sw_v=pltpu.VMEM((1, 2048), F32),
     fin_v=pltpu.VMEM((1, 512), F32),
-    pbuf=pltpu.VMEM((NZ, 8, 768), F32),
-    precv=pltpu.VMEM((NZ, 8, 768), F32),
+    pbuf=pltpu.VMEM((2 * NZ, 8, 384), F32),
+    precv=pltpu.VMEM((2, NZ, 8, 384), F32),
     qv=pltpu.VMEM((8, 768), F32),
     qs=pltpu.VMEM((8, 8, 128), F32),
     nv=pltpu.VMEM((8, 512), F32),
@@ -68,15 +73,19 @@
     op=pltpu.VMEM((NZ, 8, 512), BF16),
     orv=pltpu.VMEM((NZ, 8, 512), BF16),
     st=pltpu.VMEM((NT, 8, 128), F32),
-    lsem=pltpu.SemaphoreType.DMA((18,)),
+    len_s=pltpu.SMEM((8,), jnp.int32),
+    mix_s=pltpu.SMEM((4,), F32),
+    rt_s=pltpu.SMEM((2, 8), jnp.int32),
+    rw_s=pltpu.SMEM((2, 8), F32),
+    lsem=pltpu.SemaphoreType.DMA((21,)),
     s_wg=pltpu.SemaphoreType.DMA((NQ,)),
     r_wg=pltpu.SemaphoreType.DMA((NQ,)),
-    s_tok=pltpu.SemaphoreType.DMA((NZ,)),
-    r_tok=pltpu.SemaphoreType.DMA((NZ,)),
+    s_tok=pltpu.SemaphoreType.DMA((2 * NZ,)),
+    r_tok=pltpu.SemaphoreType.DMA((2 * NZ,)),
     s_wo=pltpu.SemaphoreType.DMA((NZ,)),
     r_wo=pltpu.SemaphoreType.DMA((NZ,)),
-    s_p=pltpu.SemaphoreType.DMA((NZ,)),
-    r_p=pltpu.SemaphoreType.DMA((NZ,)),
+    s_p=pltpu.SemaphoreType.DMA((2 * NZ,)),
+    r_p=pltpu.SemaphoreType.DMA((2 * NZ,)),
     s_n=pltpu.SemaphoreType.DMA((NQ,)),
     r_n=pltpu.SemaphoreType.DMA((NQ,)),
     s_a=pltpu.SemaphoreType.DMA((NT * NQ,)),
@@ -157,9 +166,9 @@
     zrow = pl.multiple_of(z * 32, 32)
     first = [
         pltpu.make_async_copy(tokens, s.tok_v, s.lsem.at[0]),
-        pltpu.make_async_copy(wq, s.wg.at[pl.ds(qrow, 32), pl.ds(0, 512)], s.lsem.at[1]),
-        pltpu.make_async_copy(wk, s.wg.at[pl.ds(qrow, 32), pl.ds(512, 128)], s.lsem.at[2]),
-        pltpu.make_async_copy(wv, s.wg.at[pl.ds(qrow, 32), pl.ds(640, 128)], s.lsem.at[3]),
+        pltpu.make_async_copy(wq, s.wmine.at[:, pl.ds(0, 512)], s.lsem.at[1]),
+        pltpu.make_async_copy(wk, s.wmine.at[:, pl.ds(512, 128)], s.lsem.at[2]),
+        pltpu.make_async_copy(wv, s.wmine.at[:, pl.ds(640, 128)], s.lsem.at[3]),
         pltpu.make_async_copy(wout, s.wog.at[pl.ds(zrow, 32), :], s.lsem.at[4]),
     ]
     later = [
@@ -167,6 +176,10 @@
         pltpu.make_async_copy(values, s.vbuf, s.lsem.at[6]),
         pltpu.make_async_copy(fgain, s.fg_v, s.lsem.at[7]),
         pltpu.make_async_copy(hgain, s.hg_v, s.lsem.at[8]),
+        pltpu.make_async_copy(lengths, s.len_s, s.lsem.at[17]),
+        pltpu.make_async_copy(mixw, s.mix_s, s.lsem.at[18]),
+        pltpu.make_async_copy(routing, s.rt_s, s.lsem.at[19]),
+        pltpu.make_async_copy(rweights, s.rw_s, s.lsem.at[20]),
     ]
     drow = pl.multiple_of((core * 4 + x) * 64, 64)
     dense = [
@@ -184,73 +197,90 @@
         c.start()
 
     barrier = pltpu.get_barrier_semaphore()
-    for d in range(1, NZ):
-        pl.semaphore_signal(
-            barrier, inc=1, device_id=(lax.rem(z + d, NZ) * NQ + q, y), device_id_type=MESH_ID
-        )
-    for d in range(1, NQ):
+    for d in FAR_Z:
+        for swap in range(2):
+            to = lax.rem(z + d, NZ) * NQ + x * 2 + lax.rem(core + swap, 2)
+            pl.semaphore_signal(barrier, inc=1, device_id=(to, y), device_id_type=MESH_ID)
+    for d in FAR_Q:
         pl.semaphore_signal(
             barrier, inc=1, device_id=(z * NQ + lax.rem(q + d, NQ), y), device_id_type=MESH_ID
         )
-    for d in range(1, NT):
+    for d in FAR_T:
         pl.semaphore_signal(
             barrier, inc=1, device_id=(me, lax.rem(y + d, NT)), device_id_type=MESH_ID
         )
-    for c in dense + later + last:
+    for c in dense + later:
         c.start()
     i, j = iota2((256, 256))
     s.sel[...] = jnp.where(j == (i % 32) * 8 + (i // 64) * 2 + (i // 32) % 2, 1.0, 0.0).astype(BF16)
     s.selt[...] = jnp.where(i == (j % 32) * 8 + (j // 64) * 2 + (j // 32) % 2, 1.0, 0.0).astype(BF16)
-    for c in first + dense:
+    for c in first:
         c.wait()
-    pl.semaphore_wait(barrier, NZ - 1 + NQ - 1 + NT - 1)
+    half = pl.ds(pl.multiple_of(core * 384, 384), 384)
+    s.wg[pl.ds(qrow, 32), :] = s.wmine[:, half]
+    s.tokg[z * 2 + core] = s.tok_v[:, pl.ds(pl.multiple_of(z * 256, 256), 256)]
+    pl.semaphore_wait(barrier, 2 * (NZ - 1) + NQ - 1 + NT - 1)
 
     wg_copies, tok_copies, wo_copies = [], [], []
-    for d in range(1, NZ):
-        zz = lax.rem(z + d, NZ)
-        c = remote(
-            s.tok_v.at[:, pl.ds(pl.multiple_of(zz * 256, 256), 256)], s.tokg.at[z],
-            s.s_tok.at[d], s.r_tok.at[d], zz * NQ + q, y,
-        )
+    for d in FAR_Q:
+        to = lax.rem(q + d, NQ)
+        theirs = pl.ds(pl.multiple_of(lax.rem(to, 2) * 384, 384), 384)
+        wg_copies.append(go(remote(
+            s.wmine.at[:, theirs], s.wg.at[pl.ds(qrow, 32), :], s.s_wg.at[d], s.r_wg.at[d],
+            z * NQ + to, y,
+        )))
+    for d in FAR_Z + (0,):
+        for swap in range(2):
+            if d or swap:
+                zz, k = lax.rem(z + d, NZ), d * 2 + swap
+                tok_copies.append(go(remote(
+                    s.tok_v.at[:, pl.ds(pl.multiple_of(zz * 256, 256), 256)],
+                    s.tokg.at[z * 2 + core], s.s_tok.at[k], s.r_tok.at[k],
+                    zz * NQ + x * 2 + lax.rem(core + swap, 2), y,
+                )))
+    for c in last:
         c.start()
-        tok_copies.append(c)
-    for d in range(1, NQ):
-        mine = s.wg.at[pl.ds(qrow, 32), :]
-        c = remote(mine, mine, s.s_wg.at[d], s.r_wg.at[d], z * NQ + lax.rem(q + d, NQ), y)
-        c.start()
-        wg_copies.append(c)
-    for d in range(1, NZ):
+
+    for c in tok_copies + wg_copies:
+        c.wait_recv()
+    part = dot(stacked(s.tokg, 2 * NZ), s.wg[...])
+    for i in range(2 * NZ):
+        s.pbuf[i] = part[i * 8:(i + 1) * 8]
+    p_copies = []
+    for d in FAR_Z + (0,):
+        for swap in range(2):
+            if d or swap:
+                zz, k = lax.rem(z + d, NZ), d * 2 + swap
+                cc = lax.rem(core + swap, 2)
+                p_copies.append(go(remote(
+                    s.pbuf.at[zz * 2 + cc], s.precv.at[core, z], s.s_p.at[k], s.r_p.at[k],
+                    zz * NQ + x * 2 + cc, y,
+                )))
+    for d in FAR_Z:
         mine = s.wog.at[pl.ds(zrow, 32), :]
-        c = remote(mine, mine, s.s_wo.at[d], s.r_wo.at[d], lax.rem(z + d, NZ) * NQ + q, y)
-        c.start()
-        wo_copies.append(c)
+        wo_copies.append(go(remote(
+            mine, mine, s.s_wo.at[d], s.r_wo.at[d], lax.rem(z + d, NZ) * NQ + q, y
+        )))
+    for c in dense:
+        c.wait()
     dw_copies = []
     for i in range(3):
-        for d in range(1, 4):
+        for d in FAR_X:
             mine = s.dw.at[i, pl.ds(drow, 64), :]
             k = i * 3 + d - 1
             dw_copies.append(go(remote(
                 mine, mine, s.s_dw.at[k], s.r_dw.at[k], z * NQ + lax.rem(q + 2 * d, NQ), y
             )))
-    s.tokg[z] = s.tok_v[:, pl.ds(pl.multiple_of(z * 256, 256), 256)]
-
-    for c in tok_copies + wg_copies:
-        c.wait_recv()
-    part = dot(stacked(s.tokg, NZ), s.wg[...])
-    for i in range(NZ):
-        s.pbuf[i] = part[i * 8:(i + 1) * 8]
-    p_copies = []
-    for d in range(1, NZ):
-        zz = lax.rem(z + d, NZ)
-        c = remote(s.pbuf.at[zz], s.precv.at[z], s.s_p.at[d], s.r_p.at[d], zz * NQ + q, y)
-        c.start()
-        p_copies.append(c)
-    s.precv[z] = s.pbuf[z]
+    s.precv[core, z] = s.pbuf[z * 2 + core]
     for c in p_copies:
         c.wait_recv()
-    total = s.precv[0]
-    for i in range(1, NZ):
-        total = total + s.precv[i]
+    sides = []
+    for h in range(2):
+        side = s.precv[h, 0]
+        for i in range(1, NZ):
+            side = side + s.precv[h, i]
+        sides.append(side)
+    total = jnp.concatenate(sides, axis=1)
     s.qv[...] = total.astype(BF16).astype(F32)
     for b in range(8):
         for r in range(4):
@@ -262,20 +292,20 @@
         c.wait()
     sub = lax.broadcasted_iota(jnp.int32, (8, 128), 0)
     lane = lax.broadcasted_iota(jnp.int32, (8, 128), 1)
-    half = (sub >= 4) == (lane >= 64)
+    own_half = (sub >= 4) == (lane >= 64)
     col = lax.broadcasted_iota(jnp.int32, (8, 1024), 1)
     rows1 = lax.broadcasted_iota(jnp.int32, (8, 1), 0)
     lam = jnp.zeros((8, 1), F32)
     for r in range(4):
-        lam = jnp.where(rows1 == r + 4, mixw[r], lam)
+        lam = jnp.where(rows1 == r + 4, s.mix_s[r], lam)
     weight = jnp.where(rows1 < 4, 1.0, -lam)
     for b in range(8):
-        q8 = jnp.where(half, s.qs[b], 0.0)
+        q8 = jnp.where(own_half, s.qs[b], 0.0)
         knew = s.qv[b:b + 1, 512:640]
         vnew = s.qv[b:b + 1, 640:768]
         sc = dot_nt(q8.astype(BF16), s.kbuf[b]) * 0.125
         own = jnp.sum(q8 * knew, axis=1, keepdims=True) * 0.125
-        sc = jnp.where(col < lengths[b], sc, -jnp.inf)
+        sc = jnp.where(col < s.len_s[b], sc, -jnp.inf)
         top = jnp.maximum(jnp.max(sc, axis=1, keepdims=True), own)
         e = jnp.exp(sc - top)
         eo = jnp.exp(own - top)
@@ -291,11 +321,10 @@
             s.nv[b:b + 1, r * 128:(r + 1) * 128] = n8[r:r + 1, :]
     s.ng[q] = s.nv[...].astype(BF16)
     n_copies = []
-    for d in range(1, NQ):
-        c = remote(
+    for d in FAR_Q:
+        c = go(remote(
             s.ng.at[q], s.ng.at[q], s.s_n.at[d], s.r_n.at[d], z * NQ + lax.rem(q + d, NQ), y
-        )
-        c.start()
+        ))
         n_copies.append(c)
     for c in wo_copies + n_copies:
         c.wait_recv()
@@ -303,24 +332,16 @@
     for i in range(NQ):
         s.gbuf[i] = group[i * 8:(i + 1) * 8].astype(BF16)
     a_copies = []
-    for dy in range(NT):
-        for dq in range(NQ):
+    for dq in FAR_Q + (0,):
+        for dy in FAR_T + (0,):
             if dy or dq:
                 qq = lax.rem(q + dq, NQ)
-                c = remote(
+                c = go(remote(
                     s.gbuf.at[qq], s.attr.at[y, q], s.s_a.at[dy * NQ + dq],
                     s.r_a.at[dy * NQ + dq], z * NQ + qq, lax.rem(y + dy, NT),
-                )
-                c.start()
+                ))
                 a_copies.append(c)
     s.attr[y, q] = s.gbuf[q]
-    for c in dw_copies:
-        c.wait_recv()
-    df_copies = []
-    other = me + 1 - 2 * core
-    for i in range(3):
-        mine = s.dw.at[i, pl.ds(pl.multiple_of(core * 256, 256), 256), :]
-        df_copies.append(go(remote(mine, mine, s.s_df.at[i], s.r_df.at[i], other, y)))
     for c in a_copies:
         c.wait_recv()
     parts = []
@@ -342,27 +363,30 @@
                     piece = pltpu.roll(piece, shift, 1)
                 tile = piece if tile is None else jnp.where(lane32 == k, piece, tile)
             tiles.append(tile)
-    x = s.tok_v[...].astype(F32) + jnp.concatenate(tiles, axis=1)
-    mean = jnp.mean(x, axis=1, keepdims=True)
-    xc = x - mean
+    state = s.tok_v[...].astype(F32) + jnp.concatenate(tiles, axis=1)
+    mean = jnp.mean(state, axis=1, keepdims=True)
+    xc = state - mean
     spread = jnp.mean(xc * xc, axis=1, keepdims=True)
     hidden = (xc * lax.rsqrt(spread + EPS) * s.fg_v[...]).astype(BF16)
     hid32 = hidden.astype(F32)
     s.hid[...] = hid32
 
     i, j = iota2((128, 32))
-    ones = placing(i // 8, i % 2, j % 8, routing, ONE)
+    ones = placing(i // 8, i % 2, j % 8, s.rt_s, ONE)
     place = jnp.where((i // 2) % 4 == j // 8, ones, 0.0).astype(BF16)
     quarters = jnp.concatenate([hid32[:, t * 512:(t + 1) * 512] for t in range(4)], axis=0)
     packed = dot(place, quarters.astype(BF16))
     for e in range(16):
         s.pk[e] = packed[e * 8:(e + 1) * 8].astype(BF16)
     dp_copies = []
-    for d in range(1, 32):
-        to = lax.rem(chip + d, 32)
-        dp_copies.append(go(remote(
-            s.pk.at[to // 2], s.rows.at[0, chip], s.s_dp.at[d], s.r_dp.at[d], to * 2 + core, y
-        )))
+    for dx in FAR_X + (0,):
+        for dz in FAR_Z + (0,):
+            if dx or dz:
+                to, k = lax.rem(z + dz, NZ) * 4 + lax.rem(x + dx, 4), dz * 4 + dx
+                dp_copies.append(go(remote(
+                    s.pk.at[to // 2], s.rows.at[0, chip], s.s_dp.at[k], s.r_dp.at[k],
+                    to * 2 + core, y,
+                )))
     s.rows[0, chip] = s.pk[chip // 2]
 
     s.dg[z] = s.hid[:, pl.ds(pl.multiple_of(y * 512, 512), 512)].astype(BF16)
@@ -370,29 +394,21 @@
         go(remote(
             s.dg.at[z], s.dg.at[z], s.s_dg.at[d], s.r_dg.at[d], lax.rem(z + d, NZ) * NQ + q, y
         ))
-        for d in range(1, NZ)
-    ]
+        for d in FAR_Z
+    ]
+    for c in dw_copies:
+        c.wait_recv()
+    other = me + 1 - 2 * core
+    df_copies = []
+    for i in range(3):
+        mine = s.dw.at[i, pl.ds(pl.multiple_of(core * 256, 256), 256), :]
+        df_copies.append(go(remote(mine, mine, s.s_df.at[i], s.r_df.at[i], other, y)))
     for c in last:
         c.wait()
     i, j = iota2((32, 128))
-    shares = placing(j // 8, j % 2, i % 8, routing, rweights)
+    shares = placing(j // 8, j % 2, i % 8, s.rt_s, s.rw_s)
     shares = jnp.where((j // 2) % 4 == i // 8, shares, 0.0)
     switch = 1.0 / (1.0 + jnp.exp(-jnp.sum(hid32 * s.sw_v[...], axis=1, keepdims=True)))
-
-    for c in df_copies + dg_copies:
-        c.wait_recv()
-    group = stacked(s.dg, NZ)
-    for k in range(2):
-        part = dot_nt(group, s.dw[k]).astype(BF16)
-        for t in range(NT):
-            s.gp[t, :, k * 512:(k + 1) * 512] = part[t * 16:(t + 1) * 16]
-    gr_copies = []
-    for d in range(1, NT):
-        to = lax.rem(y + d, NT)
-        gr_copies.append(go(remote(
-            s.gp.at[to], s.gr.at[y], s.s_gr.at[d], s.r_gr.at[d], me, to
-        )))
-    s.gr[y] = s.gp[y]
 
     def expert_half(h):
         block = dot(s.sel[...], jnp.concatenate(
@@ -405,45 +421,34 @@
                 s.hg.at[h, y], s.hg.at[h, y], s.s_hg.at[h * NT + d], s.r_hg.at[h * NT + d],
                 me, lax.rem(y + d, NT),
             ))
-            for d in range(1, NT)
+            for d in FAR_T
         ]
 
     for c in dp_copies:
         c.wait_recv()
     swap = go(remote(s.rows.at[0], s.rows.at[1], s.s_sw.at[0], s.r_sw.at[0], other, y))
     hg_copies = [expert_half(0)]
-
-    for c in gr_copies:
-        c.wait_recv()
-    pre = s.gr[0].astype(F32)
-    for t in range(1, NT):
-        pre = pre + s.gr[t].astype(F32)
-    s.dh[y] = (silu(pre[:, :512]) * pre[:, 512:]).astype(BF16)
-    dh_copies = [
-        go(remote(
-            s.dh.at[y], s.dh.at[y], s.s_dh.at[d], s.r_dh.at[d], me, lax.rem(y + d, NT)
-        ))
-        for d in range(1, NT)
-    ]
-
     swap.wait_recv()
     hg_copies.append(expert_half(1))
 
-    for c in dh_copies:
-        c.wait_recv()
-    part = dot(jnp.concatenate([s.dh[t] for t in range(NT)], axis=0), s.dw[2])
-    for i in range(NZ):
-        s.op[i] = part[i * 8:(i + 1) * 8].astype(BF16)
-    or_copies = []
-    for d in range(1, NZ):
-        to = lax.rem(z + d, NZ)
-        or_copies.append(go(remote(
-            s.op.at[to], s.orv.at[z], s.s_or.at[d], s.r_or.at[d], to * NQ + q, y
+    for c in df_copies + dg_copies:
+        c.wait_recv()
+    group = stacked(s.dg, NZ)
+    for k in range(2):
+        part = dot_nt(group, s.dw[k]).astype(BF16)
+        for t in range(NT):
+            s.gp[t, :, k * 512:(k + 1) * 512] = part[t * 16:(t + 1) * 16]
+    gr_copies = []
+    for d in FAR_T:
+        to = lax.rem(y + d, NT)
+        gr_copies.append(go(remote(
+            s.gp.at[to], s.gr.at[y], s.s_gr.at[d], s.r_gr.at[d], me, to
         )))
-    s.orv[z] = s.op[z]
+    s.gr[y] = s.gp[y]
 
     rt_copies = []
-    for h in range(2):
+
+    def give_back(h):
         for c in hg_copies[h]:
             c.wait_recv()
         acc = dot(s.hg[h, 0], s.ed[0:352])
@@ -455,15 +460,44 @@
         for i in range(32):
             s.rb[h, i] = back[i * 8:(i + 1) * 8].astype(BF16)
         there = core if h == 0 else 1 - core
-        for d in range(32):
-            to = lax.rem(chip + d, 32)
-            if h or d:
-                k = h * 32 + d
-                rt_copies.append(go(remote(
-                    s.rb.at[h, to], s.ret.at[me], s.s_rt.at[k], s.r_rt.at[k], to * 2 + there, y
-                )))
-            else:
-                s.ret[me] = s.rb[0, chip]
+        for dx in FAR_X + (0,):
+            for dz in FAR_Z + (0,):
+                to = lax.rem(z + dz, NZ) * 4 + lax.rem(x + dx, 4)
+                k = h * 32 + dz * 4 + dx
+                if h or dx or dz:
+                    rt_copies.append(go(remote(
+                        s.rb.at[h, to], s.ret.at[me], s.s_rt.at[k], s.r_rt.at[k],
+                        to * 2 + there, y,
+                    )))
+                else:
+                    s.ret[me] = s.rb[0, chip]
+
+    give_back(0)
+    for c in gr_copies:
+        c.wait_recv()
+    pre = s.gr[0].astype(F32)
+    for t in range(1, NT):
+        pre = pre + s.gr[t].astype(F32)
+    s.dh[y] = (silu(pre[:, :512]) * pre[:, 512:]).astype(BF16)
+    dh_copies = [
+        go(remote(
+            s.dh.at[y], s.dh.at[y], s.s_dh.at[d], s.r_dh.at[d], me, lax.rem(y + d, NT)
+        ))
+        for d in FAR_T
+    ]
+    give_back(1)
+    for c in dh_copies:
+        c.wait_recv()
+    part = dot(jnp.concatenate([s.dh[t] for t in range(NT)], axis=0), s.dw[2])
+    for i in range(NZ):
+        s.op[i] = part[i * 8:(i + 1) * 8].astype(BF16)
+    or_copies = []
+    for d in FAR_Z:
+        to = lax.rem(z + d, NZ)
+        or_copies.append(go(remote(
+            s.op.at[to], s.orv.at[z], s.s_or.at[d], s.r_or.at[d], to * NQ + q, y
+        )))
+    s.orv[z] = s.op[z]
 
     for c in or_copies:
         c.wait_recv()
@@ -493,8 +527,10 @@
         go(remote(
             s.st.at[y], s.st.at[y], s.s_st.at[d], s.r_st.at[d], me, lax.rem(y + d, NT)
         ))
-        for d in range(1, NT)
-    ]
+        for d in FAR_T
+    ]
+    for c in sent:
+        c.wait_send()
     for c in st_copies:
         c.wait_recv()
     stats = s.st[0] + s.st[1] + s.st[2] + s.st[3]
@@ -502,8 +538,6 @@
     spread = stats[:, 64:65] / 2048 - mean * mean
     result = (combined - mean) * lax.rsqrt(spread + EPS) * s.fin_v[...]
     out[...] = result.astype(BF16)
-    for c in tok_copies + wg_copies + wo_copies + p_copies + n_copies + a_copies + sent:
-        c.wait_send()
 
 
 def body(
@@ -512,11 +546,10 @@
     dense_up, dense_down, switch_vector, final_gain,
 ):
     hbm = pl.BlockSpec(memory_space=pltpu.HBM)
-    smem = pl.BlockSpec(memory_space=pltpu.SMEM)
     return pl.pallas_call(
         layer_kernel,
         out_shape=jax.ShapeDtypeStruct((8, 512), BF16),
-        in_specs=[smem] * 4 + [hbm] * 17,
+        in_specs=[hbm] * 21,
         out_specs=pl.BlockSpec(memory_space=pltpu.VMEM),
         scratch_shapes=list(SCRATCH.values()),
         compiler_params=pltpu.CompilerParams(

time: 74.9 us -> 70.3 us (0.939)
  Pallas kernels: 73.5 us -> 68.3 us
    pallas_call x1, Pallas kernels: 73.5 us -> 68.3 us  [body(): pl.pallas_call(layer_kernel, out_shape=jax.ShapeDtypeStruct((8, 512), BF1...]
where the time goes in v3:
time: 70.3 us; the launch traced here: 69.6 us
  Pallas kernels  68.3 us (97%)
  local copies, waits for them, and re-layouts  1.3 us (2%)
    pallas_call x1, Pallas kernels, body(): pl.pallas_call(layer_kernel, out_shape=jax.ShapeDtypeStruct((8, 512), BF1...  68.3 us

profile of v3, /device:TPU:1, one launch (start us, length us, event | category | flops | bytes accessed | tf_op | source)
XLA Modules:
  0.0 69.6 jit_solution(9732159904460937743)
XLA Ops:
  0.0 68.3 %layer.1 = bf16[8,512]{1,0:T(8,128)(2,1)} custom-call(s32[8]{0:T(128)} %lengths.1, f32[4]{0:T(128)} %mixw.1, s32[2,8]{1,0:T(2,128)} %bitcast.29, f32[2,8]{1,0:T(2,128)} %bitcast.30, bf16[8,2048]{1,0:T(8,128)(2,1)} %tokens.1, bf16[8,1024,128]{2,1,0:T(8,128)(2,1)} %bitcast.18, bf16[8,1024,128]{2,1,0:T(8,128)(2,1)} %bitcast.19, bf16[32,512]{1,0:T(8,128)(2,1)} %wq.1, ...), custom_call_target="tpu_custom_call" | custom-call | tf_op jit(solution)/shard_map/layer/pallas_call | solution.py:549
  68.3 1.3 %copy.23 = bf16[8,512]{1,0:T(8,128)(2,1)} copy(bf16[8,512]{1,0:T(8,128)(2,1)} %layer.1) | data formatting | bytes 16384

commit v4 on v3

--- a/solution.py
+++ b/solution.py
@@ -59,12 +59,12 @@
     ed=pltpu.VMEM((1408, 512), BF16),
     dw=pltpu.VMEM((3, 512, 512), BF16),
     hid=pltpu.VMEM((8, 2048), F32),
-    sel=pltpu.VMEM((256, 256), BF16),
-    selt=pltpu.VMEM((256, 256), BF16),
+    sel=pltpu.VMEM((128, 128), BF16),
+    selt=pltpu.VMEM((128, 128), BF16),
     pk=pltpu.VMEM((16, 8, 512), BF16),
-    rows=pltpu.VMEM((2, 32, 8, 512), BF16),
-    hg=pltpu.VMEM((2, NT, 64, 352), BF16),
-    rb=pltpu.VMEM((2, 32, 8, 128), BF16),
+    rows=pltpu.VMEM((4, 16, 8, 512), BF16),
+    hg=pltpu.VMEM((4, NT, 32, 352), BF16),
+    rb=pltpu.VMEM((4, 16, 8, 128), BF16),
     ret=pltpu.VMEM((64, 8, 128), BF16),
     dg=pltpu.VMEM((NZ, 8, 512), BF16),
     gp=pltpu.VMEM((NT, 16, 1024), BF16),
@@ -94,10 +94,12 @@
     r_dw=pltpu.SemaphoreType.DMA((9,)),
     s_df=pltpu.SemaphoreType.DMA((3,)),
     r_df=pltpu.SemaphoreType.DMA((3,)),
-    s_dp=pltpu.SemaphoreType.DMA((32,)),
-    r_dp=pltpu.SemaphoreType.DMA((32,)),
-    s_sw=pltpu.SemaphoreType.DMA((1,)),
-    r_sw=pltpu.SemaphoreType.DMA((1,)),
+    s_dp=pltpu.SemaphoreType.DMA((2 * NZ,)),
+    r_dp=pltpu.SemaphoreType.DMA((2 * NZ,)),
+    s_fx=pltpu.SemaphoreType.DMA((2 * NZ,)),
+    r_fx=pltpu.SemaphoreType.DMA((2 * NZ,)),
+    s_sw=pltpu.SemaphoreType.DMA((2,)),
+    r_sw=pltpu.SemaphoreType.DMA((2,)),
     s_dg=pltpu.SemaphoreType.DMA((NZ,)),
     r_dg=pltpu.SemaphoreType.DMA((NZ,)),
     s_gr=pltpu.SemaphoreType.DMA((NT,)),
@@ -106,8 +108,8 @@
     r_dh=pltpu.SemaphoreType.DMA((NT,)),
     s_or=pltpu.SemaphoreType.DMA((NZ,)),
     r_or=pltpu.SemaphoreType.DMA((NZ,)),
-    s_hg=pltpu.SemaphoreType.DMA((2 * NT,)),
-    r_hg=pltpu.SemaphoreType.DMA((2 * NT,)),
+    s_hg=pltpu.SemaphoreType.DMA((4 * NT,)),
+    r_hg=pltpu.SemaphoreType.DMA((4 * NT,)),
     s_rt=pltpu.SemaphoreType.DMA((64,)),
     r_rt=pltpu.SemaphoreType.DMA((64,)),
     s_st=pltpu.SemaphoreType.DMA((NT,)),
@@ -211,9 +213,9 @@
         )
     for c in dense + later:
         c.start()
-    i, j = iota2((256, 256))
-    s.sel[...] = jnp.where(j == (i % 32) * 8 + (i // 64) * 2 + (i // 32) % 2, 1.0, 0.0).astype(BF16)
-    s.selt[...] = jnp.where(i == (j % 32) * 8 + (j // 64) * 2 + (j // 32) % 2, 1.0, 0.0).astype(BF16)
+    i, j = iota2((128, 128))
+    s.sel[...] = jnp.where(j == (i % 16) * 8 + (i // 32) * 2 + (i // 16) % 2, 1.0, 0.0).astype(BF16)
+    s.selt[...] = jnp.where(i == (j % 16) * 8 + (j // 32) * 2 + (j // 16) % 2, 1.0, 0.0).astype(BF16)
     for c in first:
         c.wait()
     half = pl.ds(pl.multiple_of(core * 384, 384), 384)
@@ -299,26 +301,37 @@
     for r in range(4):
         lam = jnp.where(rows1 == r + 4, s.mix_s[r], lam)
     weight = jnp.where(rows1 < 4, 1.0, -lam)
-    for b in range(8):
-        q8 = jnp.where(own_half, s.qs[b], 0.0)
-        knew = s.qv[b:b + 1, 512:640]
-        vnew = s.qv[b:b + 1, 640:768]
-        sc = dot_nt(q8.astype(BF16), s.kbuf[b]) * 0.125
-        own = jnp.sum(q8 * knew, axis=1, keepdims=True) * 0.125
-        sc = jnp.where(col < s.len_s[b], sc, -jnp.inf)
-        top = jnp.maximum(jnp.max(sc, axis=1, keepdims=True), own)
-        e = jnp.exp(sc - top)
-        eo = jnp.exp(own - top)
-        scale = weight / (jnp.sum(e, axis=1, keepdims=True) + eo)
-        t = e * scale
-        mix = (t + pltpu.roll(t, 4, 0)).astype(BF16)
-        to = jnp.broadcast_to(eo * scale, (8, 128))
-        mix_own = (to + pltpu.roll(to, 4, 0)).astype(BF16).astype(F32)
-        ho = dot(mix, s.vbuf[b]) + mix_own * vnew
-        square = jnp.mean(ho * ho, axis=1, keepdims=True)
-        n8 = ho * lax.rsqrt(square + EPS) * s.hg_v[...]
-        for r in range(4):
-            s.nv[b:b + 1, r * 128:(r + 1) * 128] = n8[r:r + 1, :]
+    empty = jnp.zeros((8, 128), F32)
+    for b in range(0, 8, 2):
+        pair = (b, b + 1)
+        q8 = [jnp.where(own_half, s.qs[i], 0.0) for i in pair]
+        wide = jnp.concatenate(
+            [jnp.concatenate([q8[0], empty], 1), jnp.concatenate([empty, q8[1]], 1)], 0
+        )
+        both = jnp.concatenate([s.kbuf[i] for i in pair], axis=1)
+        scores = dot_nt(wide.astype(BF16), both) * 0.125
+        mixes, owns = [], []
+        for k, i in enumerate(pair):
+            sc = scores[k * 8:(k + 1) * 8]
+            own = jnp.sum(q8[k] * s.qv[i:i + 1, 512:640], axis=1, keepdims=True) * 0.125
+            sc = jnp.where(col < s.len_s[i], sc, -jnp.inf)
+            top = jnp.maximum(jnp.max(sc, axis=1, keepdims=True), own)
+            e = jnp.exp(sc - top)
+            eo = jnp.exp(own - top)
+            scale = weight / (jnp.sum(e, axis=1, keepdims=True) + eo)
+            t = e * scale
+            mixes.append(t + pltpu.roll(t, 4, 0))
+            to = jnp.broadcast_to(eo * scale, (8, 128))
+            mix_own = (to + pltpu.roll(to, 4, 0)).astype(BF16).astype(F32)
+            owns.append(mix_own * s.qv[i:i + 1, 640:768])
+        both = jnp.concatenate([s.vbuf[i] for i in pair], axis=1)
+        heads = dot(jnp.concatenate(mixes, axis=0).astype(BF16), both)
+        for k, i in enumerate(pair):
+            ho = heads[k * 8:(k + 1) * 8, k * 128:(k + 1) * 128] + owns[k]
+            square = jnp.mean(ho * ho, axis=1, keepdims=True)
+            n8 = ho * lax.rsqrt(square + EPS) * s.hg_v[...]
+            for r in range(4):
+                s.nv[i:i + 1, r * 128:(r + 1) * 128] = n8[r:r + 1, :]
     s.ng[q] = s.nv[...].astype(BF16)
     n_copies = []
     for d in FAR_Q:
@@ -342,6 +355,13 @@
                 ))
                 a_copies.append(c)
     s.attr[y, q] = s.gbuf[q]
+    for c in dw_copies:
+        c.wait_recv()
+    other = me + 1 - 2 * core
+    df_copies = []
+    for i in range(3):
+        mine = s.dw.at[i, pl.ds(pl.multiple_of(core * 256, 256), 256), :]
+        df_copies.append(go(remote(mine, mine, s.s_df.at[i], s.r_df.at[i], other, y)))
     for c in a_copies:
         c.wait_recv()
     parts = []
@@ -371,6 +391,13 @@
     hid32 = hidden.astype(F32)
     s.hid[...] = hid32
 
+    s.dg[z] = s.hid[:, pl.ds(pl.multiple_of(y * 512, 512), 512)].astype(BF16)
+    dg_copies = [
+        go(remote(
+            s.dg.at[z], s.dg.at[z], s.s_dg.at[d], s.r_dg.at[d], lax.rem(z + d, NZ) * NQ + q, y
+        ))
+        for d in FAR_Z
+    ]
     i, j = iota2((128, 32))
     ones = placing(i // 8, i % 2, j % 8, s.rt_s, ONE)
     place = jnp.where((i // 2) % 4 == j // 8, ones, 0.0).astype(BF16)
@@ -378,31 +405,30 @@
     packed = dot(place, quarters.astype(BF16))
     for e in range(16):
         s.pk[e] = packed[e * 8:(e + 1) * 8].astype(BF16)
-    dp_copies = []
-    for dx in FAR_X + (0,):
-        for dz in FAR_Z + (0,):
-            if dx or dz:
-                to, k = lax.rem(z + dz, NZ) * 4 + lax.rem(x + dx, 4), dz * 4 + dx
-                dp_copies.append(go(remote(
-                    s.pk.at[to // 2], s.rows.at[0, chip], s.s_dp.at[k], s.r_dp.at[k],
-                    to * 2 + core, y,
-                )))
-    s.rows[0, chip] = s.pk[chip // 2]
-
-    s.dg[z] = s.hid[:, pl.ds(pl.multiple_of(y * 512, 512), 512)].astype(BF16)
-    dg_copies = [
-        go(remote(
-            s.dg.at[z], s.dg.at[z], s.s_dg.at[d], s.r_dg.at[d], lax.rem(z + d, NZ) * NQ + q, y
-        ))
-        for d in FAR_Z
-    ]
-    for c in dw_copies:
-        c.wait_recv()
-    other = me + 1 - 2 * core
-    df_copies = []
-    for i in range(3):
-        mine = s.dw.at[i, pl.ds(pl.multiple_of(core * 256, 256), 256), :]
-        df_copies.append(go(remote(mine, mine, s.s_df.at[i], s.r_df.at[i], other, y)))
+    dp_copies = {}
+    for dz in FAR_Z + (0,):
+        for side in range(2):
+            if dz or side:
+                to, k = lax.rem(z + dz, NZ), dz * 2 + side
+                tx = 3 - x if side else x
+                dp_copies[k] = go(remote(
+                    s.pk.at[to * 2 + tx // 2], s.rows.at[0, z * 2 + side], s.s_dp.at[k],
+                    s.r_dp.at[k], to * NQ + tx * 2 + core, y,
+                ))
+    s.rows[0, z * 2] = s.pk[z * 2 + x // 2]
+    beside = z * NQ + (x + 1 - 2 * lax.rem(x, 2)) * 2 + core
+    fx_copies = []
+
+    def forward(dz, side):
+        k = dz * 2 + side
+        if k:
+            dp_copies[k].wait_recv()
+        at = lax.rem(z + NZ - dz, NZ) * 2 + side
+        fx_copies.append(go(remote(
+            s.rows.at[0, at], s.rows.at[2, at], s.s_fx.at[k], s.r_fx.at[k], beside, y
+        )))
+
+    forward(0, 0)
     for c in last:
         c.wait()
     i, j = iota2((32, 128))
@@ -410,10 +436,10 @@
     shares = jnp.where((j // 2) % 4 == i // 8, shares, 0.0)
     switch = 1.0 / (1.0 + jnp.exp(-jnp.sum(hid32 * s.sw_v[...], axis=1, keepdims=True)))
 
-    def expert_half(h):
+    def expert_part(h):
         block = dot(s.sel[...], jnp.concatenate(
-            [s.rows[h, i].astype(F32) for i in range(32)], axis=0).astype(BF16)).astype(BF16)
-        wide = jnp.concatenate([block[t * 64:(t + 1) * 64] for t in range(4)], axis=1)
+            [s.rows[h, i].astype(F32) for i in range(16)], axis=0).astype(BF16)).astype(BF16)
+        wide = jnp.concatenate([block[t * 32:(t + 1) * 32] for t in range(4)], axis=1)
         gate, up = dot_nt(wide, s.eg[...]), dot_nt(wide, s.eu[...])
         s.hg[h, y] = (silu(gate) * up).astype(BF16)
         return [
@@ -424,13 +450,9 @@
             for d in FAR_T
         ]
 
-    for c in dp_copies:
-        c.wait_recv()
-    swap = go(remote(s.rows.at[0], s.rows.at[1], s.s_sw.at[0], s.r_sw.at[0], other, y))
-    hg_copies = [expert_half(0)]
-    swap.wait_recv()
-    hg_copies.append(expert_half(1))
-
+    for dz in FAR_Z[:6]:
+        for side in range(2):
+            forward(dz, side)
     for c in df_copies + dg_copies:
         c.wait_recv()
     group = stacked(s.dg, NZ)
@@ -445,34 +467,20 @@
             s.gp.at[to], s.gr.at[y], s.s_gr.at[d], s.r_gr.at[d], me, to
         )))
     s.gr[y] = s.gp[y]
-
-    rt_copies = []
-
-    def give_back(h):
-        for c in hg_copies[h]:
-            c.wait_recv()
-        acc = dot(s.hg[h, 0], s.ed[0:352])
-        for t in range(1, NT):
-            acc = acc + dot(s.hg[h, t], s.ed[t * 352:(t + 1) * 352])
-        acc = acc.astype(BF16)
-        tall = jnp.concatenate([acc[:, t * 128:(t + 1) * 128] for t in range(4)], axis=0)
-        back = dot(s.selt[...], tall)
-        for i in range(32):
-            s.rb[h, i] = back[i * 8:(i + 1) * 8].astype(BF16)
-        there = core if h == 0 else 1 - core
-        for dx in FAR_X + (0,):
-            for dz in FAR_Z + (0,):
-                to = lax.rem(z + dz, NZ) * 4 + lax.rem(x + dx, 4)
-                k = h * 32 + dz * 4 + dx
-                if h or dx or dz:
-                    rt_copies.append(go(remote(
-                        s.rb.at[h, to], s.ret.at[me], s.s_rt.at[k], s.r_rt.at[k],
-                        to * 2 + there, y,
-                    )))
-                else:
-                    s.ret[me] = s.rb[0, chip]
-
-    give_back(0)
+    for dz in FAR_Z[6:] + (0,):
+        for side in range(2):
+            if dz or side:
+                forward(dz, side)
+    swap0 = go(remote(s.rows.at[0], s.rows.at[1], s.s_sw.at[0], s.r_sw.at[0], other, y))
+    hg_copies = [expert_part(0)]
+    swap0.wait_recv()
+    hg_copies.append(expert_part(1))
+    for c in fx_copies:
+        c.wait_recv()
+    swap1 = go(remote(s.rows.at[2], s.rows.at[3], s.s_sw.at[1], s.r_sw.at[1], other, y))
+    hg_copies.append(expert_part(2))
+    swap1.wait_recv()
+    hg_copies.append(expert_part(3))
     for c in gr_copies:
         c.wait_recv()
     pre = s.gr[0].astype(F32)
@@ -485,7 +493,38 @@
         ))
         for d in FAR_T
     ]
+
+    rt_copies = []
+
+    def give_back(h):
+        for c in hg_copies[h]:
+            c.wait_recv()
+        acc = dot(s.hg[h, 0], s.ed[0:352])
+        for t in range(1, NT):
+            acc = acc + dot(s.hg[h, t], s.ed[t * 352:(t + 1) * 352])
+        acc = acc.astype(BF16)
+        tall = jnp.concatenate([acc[:, t * 128:(t + 1) * 128] for t in range(4)], axis=0)
+        back = dot(s.selt[...], tall)
+        for i in range(16):
+            s.rb[h, i] = back[i * 8:(i + 1) * 8].astype(BF16)
+        there = lax.rem(core + h, 2)
+        tx = x + 1 - 2 * lax.rem(x, 2) if h >= 2 else x
+        for dz in FAR_Z + (0,):
+            for side in range(2):
+                to, k = lax.rem(z + dz, NZ), dz * 2 + side
+                if h or k:
+                    rt_copies.append(go(remote(
+                        s.rb.at[h, to * 2 + side], s.ret.at[me], s.s_rt.at[h * 16 + k],
+                        s.r_rt.at[h * 16 + k],
+                        to * NQ + (3 - tx if side else tx) * 2 + there, y,
+                    )))
+                else:
+                    s.ret[me] = s.rb[0, z * 2]
+
+    give_back(0)
     give_back(1)
+    give_back(2)
+    give_back(3)
     for c in dh_copies:
         c.wait_recv()
     part = dot(jnp.concatenate([s.dh[t] for t in range(NT)], axis=0), s.dw[2])

time: 70.3 us -> 67.6 us (0.962)
  Pallas kernels: 68.3 us -> 66.2 us
    pallas_call x1, Pallas kernels: 68.3 us -> 66.2 us  [body(): pl.pallas_call(layer_kernel, out_shape=jax.ShapeDtypeStruct((8, 512), BF1...]
where the time goes in v4:
time: 67.6 us; the launch traced here: 67.5 us
  Pallas kernels  66.2 us (98%)
  local copies, waits for them, and re-layouts  1.3 us (2%)
    pallas_call x1, Pallas kernels, body(): pl.pallas_call(layer_kernel, out_shape=jax.ShapeDtypeStruct((8, 512), BF1...  66.2 us

profile of v4, /device:TPU:1, one launch (start us, length us, event | category | flops | bytes accessed | tf_op | source)
XLA Modules:
  0.0 67.5 jit_solution(5797648339645956763)
XLA Ops:
  0.0 66.2 %layer.1 = bf16[8,512]{1,0:T(8,128)(2,1)} custom-call(s32[8]{0:T(128)} %lengths.1, f32[4]{0:T(128)} %mixw.1, s32[2,8]{1,0:T(2,128)} %bitcast.29, f32[2,8]{1,0:T(2,128)} %bitcast.30, bf16[8,2048]{1,0:T(8,128)(2,1)} %tokens.1, bf16[8,1024,128]{2,1,0:T(8,128)(2,1)} %bitcast.18, bf16[8,1024,128]{2,1,0:T(8,128)(2,1)} %bitcast.19, bf16[32,512]{1,0:T(8,128)(2,1)} %wq.1, ...), custom_call_target="tpu_custom_call" | custom-call | tf_op jit(solution)/shard_map/layer/pallas_call | solution.py:588
  66.2 1.3 %copy.23 = bf16[8,512]{1,0:T(8,128)(2,1)} copy(bf16[8,512]{1,0:T(8,128)(2,1)} %layer.1) | data formatting | bytes 16384

commit v5 on v4

--- a/solution.py
+++ b/solution.py
@@ -362,6 +362,12 @@
     for i in range(3):
         mine = s.dw.at[i, pl.ds(pl.multiple_of(core * 256, 256), 256), :]
         df_copies.append(go(remote(mine, mine, s.s_df.at[i], s.r_df.at[i], other, y)))
+    i, j = iota2((128, 32))
+    ones = placing(i // 8, i % 2, j % 8, s.rt_s, ONE)
+    place = jnp.where((i // 2) % 4 == j // 8, ones, 0.0).astype(BF16)
+    i, j = iota2((32, 128))
+    shares = placing(j // 8, j % 2, i % 8, s.rt_s, s.rw_s)
+    shares = jnp.where((j // 2) % 4 == i // 8, shares, 0.0)
     for c in a_copies:
         c.wait_recv()
     parts = []
@@ -398,9 +404,6 @@
         ))
         for d in FAR_Z
     ]
-    i, j = iota2((128, 32))
-    ones = placing(i // 8, i % 2, j % 8, s.rt_s, ONE)
-    place = jnp.where((i // 2) % 4 == j // 8, ones, 0.0).astype(BF16)
     quarters = jnp.concatenate([hid32[:, t * 512:(t + 1) * 512] for t in range(4)], axis=0)
     packed = dot(place, quarters.astype(BF16))
     for e in range(16):
@@ -431,9 +434,6 @@
     forward(0, 0)
     for c in last:
         c.wait()
-    i, j = iota2((32, 128))
-    shares = placing(j // 8, j % 2, i % 8, s.rt_s, s.rw_s)
-    shares = jnp.where((j // 2) % 4 == i // 8, shares, 0.0)
     switch = 1.0 / (1.0 + jnp.exp(-jnp.sum(hid32 * s.sw_v[...], axis=1, keepdims=True)))
 
     def expert_part(h):
@@ -587,7 +587,7 @@
     hbm = pl.BlockSpec(memory_space=pltpu.HBM)
     return pl.pallas_call(
         layer_kernel,
-        out_shape=jax.ShapeDtypeStruct((8, 512), BF16),
+        out_shape=pltpu.VMEM((8, 512), BF16),
         in_specs=[hbm] * 21,
         out_specs=pl.BlockSpec(memory_space=pltpu.VMEM),
         scratch_shapes=list(SCRATCH.values()),

time: 67.6 us -> 66.5 us (0.984)
  local copies, waits for them, and re-layouts: 1.3 us -> 0.6 us
    unnamed x1, local copies, waits for them, and re-layouts: 1.3 us -> 0.6 us
where the time goes in v5:
time: 66.5 us; the launch traced here: 66.4 us
  Pallas kernels  65.8 us (99%)
    pallas_call x1, Pallas kernels, body(): pl.pallas_call(layer_kernel, out_shape=pltpu.VMEM((8, 512), BF16), in_spe...  65.8 us

profile of v5, /device:TPU:1, one launch (start us, length us, event | category | flops | bytes accessed | tf_op | source)
XLA Modules:
  0.0 66.4 jit_solution(18067884440525561774)
XLA Ops:
  0.0 65.8 %layer.1 = bf16[8,512]{1,0:T(8,128)(2,1)S(1)} custom-call(s32[8]{0:T(128)} %lengths.1, f32[4]{0:T(128)} %mixw.1, s32[2,8]{1,0:T(2,128)} %bitcast.29, f32[2,8]{1,0:T(2,128)} %bitcast.30, bf16[8,2048]{1,0:T(8,128)(2,1)} %tokens.1, bf16[8,1024,128]{2,1,0:T(8,128)(2,1)} %bitcast.18, bf16[8,1024,128]{2,1,0:T(8,128)(2,1)} %bitcast.19, bf16[32,512]{1,0:T(8,128)(2,1)} %wq.1, ...), custom_call_target="tpu_custom_call" | custom-call | tf_op jit(solution)/shard_map/layer/pallas_call | solution.py:588
  65.8 0.6 copy.23
